TPU v7x, 512 devices: a whole 4x8x8 slice. The times are simulated.
512 devices in a mesh: ep: 32 (over z, x), tp: 16 (over y, core).
Axes of the slice: x: 4, y: 8, z: 8, core: 2. Of those that a mesh axis runs over, the one named last changes fastest.
Arguments:
- tokens: bfloat16 [1024, 4096], P(('ep', 'tp')), may hold values from -6 to 6
- lengths: int32 [1024], P('ep'), may hold values from 64 to 1024, as said below
- latent_cache: bfloat16 [1024, 1024, 256], P(('ep', 'tp')), may hold values from -6 to 6
- rope_cache: bfloat16 [1024, 1024, 64], P(('ep', 'tp')), may hold values from -1200 to 1200
- attn_gain: bfloat16 [4096], replicated, may hold values from 0.099609375 to 1.8984375
- query_weight: bfloat16 [4096, 2048], P(None, 'tp'), may hold values from -0.09375 to 0.09375
- query_rot_weight: bfloat16 [4096, 1024], P(None, 'tp'), may hold values from -0.09375 to 0.09375
- latent_weight: bfloat16 [4096, 256], P('tp'), may hold values from -0.09375 to 0.09375
- key_rot_weight: bfloat16 [4096, 64], P('tp'), may hold values from -0.09375 to 0.09375
- latent_gain: bfloat16 [256], replicated, may hold values from 0.099609375 to 1.8984375
- absorb_weight: bfloat16 [16, 128, 256], P('tp'), may hold values from -0.5 to 0.5
- value_weight: bfloat16 [16, 256, 128], P('tp'), may hold values from -0.375 to 0.375
- output_weight: bfloat16 [2048, 4096], P('tp'), may hold values from -0.125 to 0.125
- mix_gain: bfloat16 [4096], replicated, may hold values from 0.099609375 to 1.8984375
- expert_gain: bfloat16 [4096], replicated, may hold values from 0.099609375 to 1.8984375
- gate_weight: bfloat16 [32, 4096, 512], P('ep', None, 'tp'), may hold values from -0.09375 to 0.09375
- up_weight: bfloat16 [32, 4096, 512], P('ep', None, 'tp'), may hold values from -0.09375 to 0.09375
- down_weight: bfloat16 [32, 512, 4096], P('ep', 'tp'), may hold values from -0.25 to 0.25
- expert_ids: int32 [1024, 2], P('ep'), may hold values from 0 to 31, all different within a row; in each aligned block of 32 rows (0 to 31, 32 to 63, ...) at most 4 rows name the same one
- route_weights: float32 [1024, 2], P('ep'), may hold values from 0.2 to 1
Outputs:
- out: bfloat16 [1024, 4096], P('ep', 'tp')
- new_latent: bfloat16 [1024, 256], P(('ep', 'tp'))
- new_rope: bfloat16 [1024, 64], P(('ep', 'tp'))
Inputs may be any that keep to these rules, and one draw needn't show every extreme that they name: The new token sits at position lengths[b]; some sequence has exactly 1024. `expert_ids`: the experts of a row differ; among the rows of one index of ep no expert is named by more than 4 rows, a bound that some block reaches there.
All inputs are finite; a program needn't handle non-finite values.
Results may differ from a plain program's by a relative error of at most 0.023.
Values may be sent and summed in bfloat16 or wider, within the bound.
A program may use at most 64 MiB of HBM per device.

v0:
```python
import jax
import jax.numpy as jnp
from jax import lax
from jax.sharding import PartitionSpec as P

QK_NOPE = 128
QK_ROPE = 64
KEY_BLOCK = 256


norm_floor = 1e-06
rope_base = 10000.0
masked_score = -1e30


def copy_for_each(value, axis):
    copies = jnp.broadcast_to(value, (lax.axis_size(axis), *value.shape))
    return lax.all_to_all(copies, axis, split_axis=0, concat_axis=0, tiled=True)


def joined_along(tiles, dim):
    lengths = list(tiles.shape[1:])
    lengths[dim] *= tiles.shape[0]
    return jnp.moveaxis(tiles, 0, dim).reshape(lengths)


def collect(value, axis, dim):
    tiles = copy_for_each(value, axis)
    return joined_along(tiles, dim)


def cut_along(value, dim, size):
    before, after = (value.shape[:dim], value.shape[dim + 1 :])
    return jnp.moveaxis(value.reshape(*before, size, -1, *after), dim, 0)


def summed_on_arrival(value, axis, dim):
    tiles = cut_along(value, dim, lax.axis_size(axis))
    arrived = lax.all_to_all(tiles, axis, split_axis=0, concat_axis=0, tiled=True)
    return arrived.astype(jnp.float32).sum(axis=0)


def side_by_side(arrays, axis, split_dim, concat_dim, along):
    ends, at = ([], 0)
    for a in arrays[:-1]:
        at += a.shape[along]
        ends.append(at)
    both = jnp.concatenate(arrays, axis=along)
    return tuple(
        jnp.split(
            lax.all_to_all(both, axis, split_axis=split_dim, concat_axis=concat_dim, tiled=True),
            ends,
            axis=along,
        )
    )


def over_pieces(value, axis):
    tiles = lax.all_gather(value, axis).astype(jnp.float32)
    return tiles.sum(axis=0)


def normed(values, gain):
    wide = values.astype(jnp.float32)
    factor = lax.rsqrt(jnp.mean(wide * wide, axis=-1, keepdims=True) + norm_floor)
    return wide * factor * gain.astype(jnp.float32)


def rotate(values, angle_pos):
    half = values.shape[-1] // 2
    freqs = rope_base ** (-jnp.arange(half, dtype=jnp.float32) / half)
    angles = angle_pos.astype(jnp.float32)[..., None] * freqs
    cosine = jnp.cos(angles)
    sine = jnp.sin(angles)
    first_half = values[..., :half]
    second_half = values[..., half:]
    return jnp.concatenate(
        [first_half * cosine - second_half * sine, second_half * cosine + first_half * sine],
        axis=-1,
    )


def through_bf16(values):
    return lax.optimization_barrier(values.astype(jnp.bfloat16)).astype(jnp.float32)


def expert_tail(received, gate_mat, up_mat, down_mat):
    sources, slots, width = received.shape
    flat = received.reshape(sources * slots, width)
    gate = jnp.dot(flat, gate_mat, preferred_element_type=jnp.float32)
    upward = jnp.dot(flat, up_mat, preferred_element_type=jnp.float32)
    hidden = (jax.nn.silu(gate) * upward).astype(jnp.bfloat16)
    groups = lax.axis_size("tp")
    unit_group = hidden.shape[1]
    all_hidden = collect(hidden, "tp", 1)
    down_cols = lax.all_to_all(down_mat, "tp", split_axis=1, concat_axis=0, tiled=True)
    col_width = down_cols.shape[1]
    parts = jnp.einsum(
        "rgf,gfd->rgd",
        all_hidden.reshape(-1, groups, unit_group),
        down_cols.reshape(groups, unit_group, col_width),
        preferred_element_type=jnp.float32,
    )
    summed = (
        jnp.sum(through_bf16(parts), axis=1).astype(jnp.bfloat16).reshape(sources, slots, col_width)
    )
    return lax.all_to_all(summed, "ep", split_axis=0, concat_axis=0, tiled=True)


def per_device(
    tokens,
    lengths,
    latent_cache,
    rope_cache,
    attn_gain,
    query_weight,
    query_rot_weight,
    latent_weight,
    key_rot_weight,
    latent_gain,
    absorb_weight,
    value_weight,
    output_weight,
    mix_gain,
    expert_gain,
    gate_weight,
    up_weight,
    down_weight,
    expert_ids,
    route_weights,
):
    groups = lax.axis_size("tp")
    place = lax.axis_index("tp")
    own_rows = tokens.shape[0]
    width = tokens.shape[1]
    slice_width = width // groups
    heads_dev = absorb_weight.shape[0]
    latent_width = absorb_weight.shape[2]
    score_scale = (QK_NOPE + QK_ROPE) ** (-0.5)
    group_tokens = collect(tokens, "tp", 0)
    normed_in = normed(group_tokens, attn_gain).astype(jnp.bfloat16)
    q_nope = jnp.dot(normed_in, query_weight, preferred_element_type=jnp.float32).astype(
        jnp.bfloat16
    )
    q_nope = q_nope.reshape(-1, heads_dev, QK_NOPE)
    q_rot = jnp.dot(normed_in, query_rot_weight, preferred_element_type=jnp.float32).reshape(
        -1, heads_dev, QK_ROPE
    )
    q_rot = rotate(q_rot, lengths[:, None]).astype(jnp.bfloat16)
    q_latent = jnp.einsum(
        "thn,hnl->thl", q_nope, absorb_weight, preferred_element_type=jnp.float32
    ).astype(jnp.bfloat16)
    key_weights = jnp.concatenate([latent_weight, key_rot_weight], axis=1)
    slice_rows = lax.dynamic_slice_in_dim(normed_in, place * slice_width, slice_width, 1)
    key_raw = summed_on_arrival(
        jnp.dot(slice_rows, key_weights, preferred_element_type=jnp.float32).astype(jnp.bfloat16),
        "tp",
        0,
    )
    own_len = lax.dynamic_slice_in_dim(lengths, place * own_rows, own_rows, 0)
    new_latent = normed(key_raw[:, :latent_width], latent_gain).astype(jnp.bfloat16)
    new_rope = rotate(key_raw[:, latent_width:], own_len).astype(jnp.bfloat16)
    seq_lat, seq_rot = side_by_side((q_latent, q_rot), "tp", 0, 1, 2)
    own_score = (
        jnp.einsum("shl,sl->sh", seq_lat, new_latent, preferred_element_type=jnp.float32)
        + jnp.einsum("shr,sr->sh", seq_rot, new_rope, preferred_element_type=jnp.float32)
    ) * score_scale
    longest = jnp.max(own_len)
    trips = (longest + KEY_BLOCK - 1) // KEY_BLOCK

    def sweep(block_index, carry):
        top, total, summed = carry
        begin = block_index * KEY_BLOCK
        latents = lax.dynamic_slice_in_dim(latent_cache, begin, KEY_BLOCK, 1)
        rotated = lax.dynamic_slice_in_dim(rope_cache, begin, KEY_BLOCK, 1)
        scores = (
            jnp.einsum("shl,skl->shk", seq_lat, latents, preferred_element_type=jnp.float32)
            + jnp.einsum("shr,skr->shk", seq_rot, rotated, preferred_element_type=jnp.float32)
        ) * score_scale
        valid = (begin + jnp.arange(KEY_BLOCK))[None, None, :] < own_len[:, None, None]
        scores = jnp.where(valid, scores, masked_score)
        new_top = jnp.maximum(top, jnp.max(scores, axis=-1))
        factor = jnp.exp(top - new_top)
        weights = jnp.where(valid, jnp.exp(scores - new_top[..., None]), 0.0)
        total = total * factor + jnp.sum(weights, axis=-1)
        summed = summed * factor[..., None] + jnp.einsum(
            "shk,skl->shl",
            weights.astype(jnp.bfloat16),
            latents,
            preferred_element_type=jnp.float32,
        )
        return (new_top, total, summed)

    start_sum = jnp.broadcast_to(new_latent.astype(jnp.float32)[:, None, :], seq_lat.shape)
    top, total, summed = lax.fori_loop(
        0, trips, sweep, (own_score, jnp.ones_like(own_score), start_sum)
    )
    head_latent = (summed / total[..., None]).astype(jnp.bfloat16)
    group_latent = lax.all_to_all(head_latent, "tp", split_axis=1, concat_axis=0, tiled=True)
    head_values = jnp.einsum(
        "thl,hlv->thv", group_latent, value_weight, preferred_element_type=jnp.float32
    )
    head_values = head_values.astype(jnp.bfloat16).reshape(group_latent.shape[0], -1)
    partial_value = through_bf16(
        jnp.dot(head_values, output_weight, preferred_element_type=jnp.float32)
    )
    mixed = (
        over_pieces(partial_value.astype(jnp.bfloat16), "tp")
        .astype(jnp.float32)
        .astype(jnp.bfloat16)
    )
    resid = (group_tokens.astype(jnp.float32) + normed(mixed, mix_gain)).astype(jnp.bfloat16)
    expert_in = normed(resid, expert_gain).astype(jnp.bfloat16)
    experts = lax.axis_size("ep")
    topk = expert_ids.shape[1]
    routes = expert_ids.reshape(-1)
    count_routes = routes.shape[0]
    capacity = 2 * count_routes // experts
    picks = (routes[:, None] == jnp.arange(experts, dtype=jnp.int32)[None, :]).astype(jnp.int32)
    ranks = jnp.sum((jnp.cumsum(picks, axis=0) - picks) * picks, axis=1)
    target = routes * capacity + ranks
    slot_ids = jnp.arange(experts * capacity, dtype=jnp.int32)
    dispatch = jnp.sum(
        (slot_ids[:, None] == target[None, :])
        .astype(jnp.int32)
        .reshape(experts * capacity, -1, topk),
        axis=2,
    )
    dispatch = dispatch.astype(jnp.bfloat16)
    gate_mat = gate_weight[0]
    up_mat = up_weight[0]
    down_mat = down_weight[0]
    outgoing = jnp.dot(dispatch, expert_in, preferred_element_type=jnp.float32).astype(jnp.bfloat16)
    outgoing = outgoing.reshape(experts, capacity, width)
    returned = expert_tail(
        lax.all_to_all(outgoing, "ep", split_axis=0, concat_axis=0, tiled=True),
        gate_mat,
        up_mat,
        down_mat,
    )
    picked = returned.reshape(experts * capacity, slice_width)[target]
    moe_out = jnp.sum(
        picked.astype(jnp.float32).reshape(-1, topk, slice_width) * route_weights[:, :, None],
        axis=1,
    )
    resid_slice = lax.dynamic_slice_in_dim(resid, place * slice_width, slice_width, 1)
    out = (resid_slice.astype(jnp.float32) + moe_out).astype(jnp.bfloat16)
    return (out, new_latent, new_rope)


def solution(mesh):
    placed = (
        P(("ep", "tp"), None),
        P("ep"),
        P(("ep", "tp"), None, None),
        P(("ep", "tp"), None, None),
        P(),
        P(None, "tp"),
        P(None, "tp"),
        P("tp", None),
        P("tp", None),
        P(),
        P("tp", None, None),
        P("tp", None, None),
        P("tp", None),
        P(),
        P(),
        P("ep", None, "tp"),
        P("ep", None, "tp"),
        P("ep", "tp", None),
        P("ep", None),
        P("ep", None),
    )
    return jax.shard_map(
        per_device,
        mesh=mesh,
        in_specs=placed,
        out_specs=(P("ep", "tp"), P(("ep", "tp"), None), P(("ep", "tp"), None)),
        check_vma=False,
    )
```

profile of v0, /device:TPU:1, one launch (start us, length us, event | category | flops | bytes accessed | tf_op | source)
XLA Modules:
  0.0 217.6 jit_solution(7336680002364809128)
XLA Ops:
  7.2 1.7 broadcast_in_dim.32
  8.9 10.2 %all-to-all-start = ((bf16[16,2,4096]{2,1,0:T(2,128)(2,1)}), bf16[16,2,4096]{2,1,0:T(2,128)(2,1)S(1)}, u32[]{:S(2)}, u32[]{:S(2)}) async-start(bf16[16,2,4096]{2,1,0:T(2,128)(2,1)} %broadcast_in_dim.32), calls=%async_computation | async-start | bytes 524288 | tf_op jit(solution)/shard_map/all_to_all | solution.py:18
  19.1 0.7 convert_element_type.153
  19.8 0.9 copy.66
  20.6 0.7 convert_element_type.160
  21.3 9.5 %all-to-all-done = bf16[16,2,4096]{2,1,0:T(2,128)(2,1)S(1)} async-done(((bf16[16,2,4096]{2,1,0:T(2,128)(2,1)}), bf16[16,2,4096]{2,1,0:T(2,128)(2,1)S(1)}, u32[]{:S(2)}, u32[]{:S(2)}) %all-to-all-start) | async-done | bytes 262176 | tf_op jit(solution)/shard_map/all_to_all | solution.py:18
  31.5 1.4 convolution_bitcast_fusion
  32.9 1.6 fusion.18
  36.6 3.4 %all-to-all-start.1 = ((bf16[16,2,320]{2,1,0:T(2,128)(2,1)}), bf16[16,2,320]{2,1,0:T(2,128)(2,1)S(1)}, u32[]{:S(2)}, u32[]{:S(2)}) async-start(bf16[16,2,320]{2,1,0:T(2,128)(2,1)} %reshape.369), calls=%async_computation.1 | async-start | bytes 49152 | tf_op jit(solution)/shard_map/all_to_all | solution.py:51
  40.7 6.1 %all-to-all-done.1 = bf16[16,2,320]{2,1,0:T(2,128)(2,1)S(1)} async-done(((bf16[16,2,320]{2,1,0:T(2,128)(2,1)}), bf16[16,2,320]{2,1,0:T(2,128)(2,1)S(1)}, u32[]{:S(2)}, u32[]{:S(2)}) %all-to-all-start.1) | async-done | bytes 20512 | tf_op jit(solution)/shard_map/all_to_all | solution.py:51
  46.8 3.7 %all-to-all-start.2 = ((bf16[16,2,320]{2,1,0:T(2,128)(2,1)}), bf16[16,2,320]{2,1,0:T(2,128)(2,1)S(1)}, u32[]{:S(2)}, u32[]{:S(2)}) async-start(bf16[16,2,320]{2,1,0:T(2,128)(2,1)} %reshape.345), calls=%async_computation.2 | async-start | bytes 49152 | tf_op jit(solution)/shard_map/all_to_all | solution.py:39
  50.5 0.7 fusion.62
  52.2 5.7 %all-to-all-done.2 = bf16[16,2,320]{2,1,0:T(2,128)(2,1)S(1)} async-done(((bf16[16,2,320]{2,1,0:T(2,128)(2,1)}), bf16[16,2,320]{2,1,0:T(2,128)(2,1)S(1)}, u32[]{:S(2)}, u32[]{:S(2)}) %all-to-all-start.2) | async-done | bytes 20512 | tf_op jit(solution)/shard_map/all_to_all | solution.py:39
  58.8 1.7 while.14
  59.1 1.1 fusion.90
  60.6 14.6 %all_to_all.74 = bf16[2,16,256]{2,0,1:T(2,128)(2,1)S(1)} all-to-all(bf16[2,16,256]{2,0,1:T(2,128)(2,1)S(1)} %copy.69), channel_id=1, replica_groups=mesh['ep'=32,'tp'=16] {'tp'}, dimensions={1} | all-to-all | bytes 32768 | tf_op jit(solution)/shard_map/all_to_all | solution.py:199
  75.3 1.1 convolution_convert_fusion.1
  77.3 42.1 %all-gather.3.cloned.1.call-done = bf16[512,4096]{1,0:T(8,128)(2,1)} async-done(((bf16[32,4096]{1,0:T(8,128)(2,1)}), bf16[512,4096]{1,0:T(8,128)(2,1)}) %all-gather.3.cloned.1.call-update) | async-done | bytes 4194320 | tf_op jit(solution)/shard_map/all_gather | solution.py:59
  119.4 3.0 %reduce_sum.112 = bf16[32,4096]{1,0:T(8,128)(2,1)S(1)} reduce(bf16[16,32,4096]{2,1,0:T(8,128)(2,1)} %bitcast.71, bf16[]{:T(256)} %constant.82.clone.1), dimensions={0}, to_apply=%region_8.9 | reduce | flops 1966080 | bytes 4456450 | tf_op jit(solution)/shard_map/reduce_sum | solution.py:60
  124.4 1.2 reshape.348
  125.6 9.9 %all-to-all-start.4 = ((bf16[32,4,4096]{2,1,0:T(4,128)(2,1)}), bf16[32,4,4096]{2,1,0:T(4,128)(2,1)S(1)}, u32[]{:S(2)}, u32[]{:S(2)}) async-start(bf16[32,4,4096]{2,1,0:T(4,128)(2,1)} %reshape.348), calls=%async_computation.4 | async-start | bytes 2097152 | tf_op jit(solution)/shard_map/all_to_all | solution.py:236
  135.6 0.8 copy.73
  136.4 26.0 %all-to-all-done.4 = bf16[32,4,4096]{2,1,0:T(4,128)(2,1)S(1)} async-done(((bf16[32,4,4096]{2,1,0:T(4,128)(2,1)}), bf16[32,4,4096]{2,1,0:T(4,128)(2,1)S(1)}, u32[]{:S(2)}, u32[]{:S(2)}) %all-to-all-start.4) | async-done | bytes 1048608 | tf_op jit(solution)/shard_map/all_to_all | solution.py:236
  162.4 1.0 copy-done.2
  163.4 6.3 %all-to-all-start.6 = ((bf16[32,16,256]{2,0,1:T(8,128)(2,1)}), bf16[32,16,256]{2,0,1:T(8,128)(2,1)S(1)}, u32[]{:S(2)}, u32[]{:S(2)}) async-start(bf16[32,16,256]{2,0,1:T(8,128)(2,1)} %copy.73), calls=%async_computation.6 | async-start | bytes 524288 | tf_op jit(solution)/shard_map/all_to_all | solution.py:96
  169.7 1.3 reshape.349
  172.0 9.3 %all-to-all-done.6 = bf16[32,16,256]{2,0,1:T(8,128)(2,1)S(1)} async-done(((bf16[32,16,256]{2,0,1:T(8,128)(2,1)}), bf16[32,16,256]{2,0,1:T(8,128)(2,1)S(1)}, u32[]{:S(2)}, u32[]{:S(2)}) %all-to-all-start.6) | async-done | bytes 262176 | tf_op jit(solution)/shard_map/all_to_all | solution.py:96
  181.9 3.4 %all-to-all-start.5 = ((bf16[16,128,32]{1,2,0:T(8,128)(2,1)}), bf16[16,128,32]{1,2,0:T(8,128)(2,1)S(1)}, u32[]{:S(2)}, u32[]{:S(2)}) async-start(bf16[16,128,32]{1,2,0:T(8,128)(2,1)} %broadcast_in_dim.35), calls=%async_computation.5 | async-start | bytes 262144 | tf_op jit(solution)/shard_map/all_to_all | solution.py:18
  185.5 8.3 %all-to-all-done.5 = bf16[16,128,32]{1,2,0:T(8,128)(2,1)S(1)} async-done(((bf16[16,128,32]{1,2,0:T(8,128)(2,1)}), bf16[16,128,32]{1,2,0:T(8,128)(2,1)S(1)}, u32[]{:S(2)}, u32[]{:S(2)}) %all-to-all-start.5) | async-done | bytes 131104 | tf_op jit(solution)/shard_map/all_to_all | solution.py:18
  195.1 5.3 %all-to-all-start.7 = ((bf16[32,4,256]{2,1,0:T(4,128)(2,1)}), bf16[32,4,256]{2,1,0:T(4,128)(2,1)S(1)}, u32[]{:S(2)}, u32[]{:S(2)}) async-start(bf16[32,4,256]{2,1,0:T(4,128)(2,1)} %reshape.350), calls=%async_computation.7 | async-start | bytes 131072 | tf_op jit(solution)/shard_map/all_to_all | solution.py:107
  201.1 8.2 %all-to-all-done.7 = bf16[32,4,256]{2,1,0:T(4,128)(2,1)S(1)} async-done(((bf16[32,4,256]{2,1,0:T(4,128)(2,1)}), bf16[32,4,256]{2,1,0:T(4,128)(2,1)S(1)}, u32[]{:S(2)}, u32[]{:S(2)}) %all-to-all-start.7) | async-done | bytes 65568 | tf_op jit(solution)/shard_map/all_to_all | solution.py:107
  209.3 0.7 gather_fusion
  (114 shorter events, 12.7 us)
Async XLA Ops:
  7.2 68.1 %copy-start = (bf16[128,4096]{1,0:T(8,128)(2,1)S(1)}, bf16[128,4096]{1,0:T(8,128)(2,1)}, u32[]{:S(2)}) copy-start(bf16[128,4096]{1,0:T(8,128)(2,1)} %param.34) | copy-start | bytes 3145732
  7.2 25.7 %copy-start.6 = (bf16[1,128,256]{2,1,0:T(8,128)(2,1)S(1)}, bf16[1,128,256]{2,1,0:T(8,128)(2,1)}, u32[]{:S(2)}) copy-start(bf16[1,128,256]{2,1,0:T(8,128)(2,1)} %param.32) | copy-start | bytes 196612
  8.9 21.9 %all-to-all-start = ((bf16[16,2,4096]{2,1,0:T(2,128)(2,1)}), bf16[16,2,4096]{2,1,0:T(2,128)(2,1)S(1)}, u32[]{:S(2)}, u32[]{:S(2)}) async-start(bf16[16,2,4096]{2,1,0:T(2,128)(2,1)} %broadcast_in_dim.32), calls=%async_computation | async-start | bytes 524288 | tf_op jit(solution)/shard_map/all_to_all | solution.py:18
  31.2 8.8 %copy-start.14 = (bf16[256,256]{1,0:T(8,128)(2,1)S(1)}, bf16[256,256]{1,0:T(8,128)(2,1)}, u32[]{:S(2)}) copy-start(bf16[256,256]{1,0:T(8,128)(2,1)} %param.29) | copy-start | bytes 393220
  31.3 19.2 %copy-start.13 = (s32[32]{0:T(128)S(1)}, s32[32]{0:T(128)}, u32[]{:S(2)}) copy-start(s32[32]{0:T(128)} %param.23) | copy-start | bytes 388
  31.3 20.6 %copy-start.15 = (bf16[256]{0:T(256)(128)(2,1)S(1)}, bf16[256]{0:T(256)(128)(2,1)}, u32[]{:S(2)}) copy-start(bf16[256]{0:T(256)(128)(2,1)} %param.31) | copy-start | bytes 1540
  31.4 27.3 %copy-start.1 = (bf16[2,1024,256]{2,1,0:T(8,128)(2,1)S(1)}, bf16[2,1024,256]{2,1,0:T(8,128)(2,1)}, u32[]{:S(2)}) copy-start(bf16[2,1024,256]{2,1,0:T(8,128)(2,1)} %param.24) | copy-start | bytes 3145732
  36.6 10.2 %all-to-all-start.1 = ((bf16[16,2,320]{2,1,0:T(2,128)(2,1)}), bf16[16,2,320]{2,1,0:T(2,128)(2,1)S(1)}, u32[]{:S(2)}, u32[]{:S(2)}) async-start(bf16[16,2,320]{2,1,0:T(2,128)(2,1)} %reshape.369), calls=%async_computation.1 | async-start | bytes 49152 | tf_op jit(solution)/shard_map/all_to_all | solution.py:51
  46.8 11.2 %all-to-all-start.2 = ((bf16[16,2,320]{2,1,0:T(2,128)(2,1)}), bf16[16,2,320]{2,1,0:T(2,128)(2,1)S(1)}, u32[]{:S(2)}, u32[]{:S(2)}) async-start(bf16[16,2,320]{2,1,0:T(2,128)(2,1)} %reshape.345), calls=%async_computation.2 | async-start | bytes 49152 | tf_op jit(solution)/shard_map/all_to_all | solution.py:39
  50.5 68.9 %all-gather.3.cloned.1.call-start = ((), (), s32[]{:S(2)}) async-start(), calls=%async_computation.8 | async-start | bytes 4456448 | tf_op jit(solution)/shard_map/all_gather | solution.py:59
  58.3 0.6 copy-start.10
  58.7 16.5 %copy-start.7 = (bf16[1,256,128]{2,1,0:T(8,128)(2,1)S(1)}, bf16[1,256,128]{2,1,0:T(8,128)(2,1)}, u32[]{:S(2)}) copy-start(bf16[1,256,128]{2,1,0:T(8,128)(2,1)} %param.33) | copy-start | bytes 196612
  58.7 17.6 %copy-start.8 = (bf16[4096]{0:T(1024)(128)(2,1)S(1)}, bf16[4096]{0:T(1024)(128)(2,1)}, u32[]{:S(2)}) copy-start(bf16[4096]{0:T(1024)(128)(2,1)} %param.35) | copy-start | bytes 24580
  58.8 17.6 %copy-start.11 = (s32[32,2]{0,1:T(2,128)S(1)}, s32[32,2]{0,1:T(2,128)}, u32[]{:S(2)}) copy-start(s32[32,2]{0,1:T(2,128)} %param.40) | copy-start | bytes 772
  60.5 16.6 %copy-start.9 = (bf16[4096]{0:T(1024)(128)(2,1)S(1)}, bf16[4096]{0:T(1024)(128)(2,1)}, u32[]{:S(2)}) copy-start(bf16[4096]{0:T(1024)(128)(2,1)} %param.36) | copy-start | bytes 24580
  124.4 11.2 %copy-start.3 = (bf16[1,32,4096]{2,1,0:T(8,128)(2,1)S(1)}, bf16[1,32,4096]{2,1,0:T(8,128)(2,1)}, u32[]{:S(2)}) copy-start(bf16[1,32,4096]{2,1,0:T(8,128)(2,1)} %param.39) | copy-start | bytes 786436
  125.6 36.8 %all-to-all-start.4 = ((bf16[32,4,4096]{2,1,0:T(4,128)(2,1)}), bf16[32,4,4096]{2,1,0:T(4,128)(2,1)S(1)}, u32[]{:S(2)}, u32[]{:S(2)}) async-start(bf16[32,4,4096]{2,1,0:T(4,128)(2,1)} %reshape.348), calls=%async_computation.4 | async-start | bytes 2097152 | tf_op jit(solution)/shard_map/all_to_all | solution.py:236
  135.5 35.5 %copy-start.4 = (bf16[1,4096,32]{1,2,0:T(8,128)(2,1)S(1)}, bf16[1,4096,32]{1,2,0:T(8,128)(2,1)}, u32[]{:S(2)}) copy-start(bf16[1,4096,32]{1,2,0:T(8,128)(2,1)} %param.37) | copy-start | bytes 786436
  136.4 35.1 %copy-start.5 = (bf16[1,4096,32]{1,2,0:T(8,128)(2,1)S(1)}, bf16[1,4096,32]{1,2,0:T(8,128)(2,1)}, u32[]{:S(2)}) copy-start(bf16[1,4096,32]{1,2,0:T(8,128)(2,1)} %param.38) | copy-start | bytes 786436
  162.4 1.0 copy-start.2
  163.4 17.9 %all-to-all-start.6 = ((bf16[32,16,256]{2,0,1:T(8,128)(2,1)}), bf16[32,16,256]{2,0,1:T(8,128)(2,1)S(1)}, u32[]{:S(2)}, u32[]{:S(2)}) async-start(bf16[32,16,256]{2,0,1:T(8,128)(2,1)} %copy.73), calls=%async_computation.6 | async-start | bytes 524288 | tf_op jit(solution)/shard_map/all_to_all | solution.py:96
  171.5 28.9 %copy-start.12 = (f32[32,2]{0,1:T(2,128)S(1)}, f32[32,2]{0,1:T(2,128)}, u32[]{:S(2)}) copy-start(f32[32,2]{0,1:T(2,128)} %param.41) | copy-start | bytes 772
  181.9 11.9 %all-to-all-start.5 = ((bf16[16,128,32]{1,2,0:T(8,128)(2,1)}), bf16[16,128,32]{1,2,0:T(8,128)(2,1)S(1)}, u32[]{:S(2)}, u32[]{:S(2)}) async-start(bf16[16,128,32]{1,2,0:T(8,128)(2,1)} %broadcast_in_dim.35), calls=%async_computation.5 | async-start | bytes 262144 | tf_op jit(solution)/shard_map/all_to_all | solution.py:18
  195.1 14.2 %all-to-all-start.7 = ((bf16[32,4,256]{2,1,0:T(4,128)(2,1)}), bf16[32,4,256]{2,1,0:T(4,128)(2,1)S(1)}, u32[]{:S(2)}, u32[]{:S(2)}) async-start(bf16[32,4,256]{2,1,0:T(4,128)(2,1)} %reshape.350), calls=%async_computation.7 | async-start | bytes 131072 | tf_op jit(solution)/shard_map/all_to_all | solution.py:107
Sparse Core Ops, SparseCore 0:
  76.5 42.8 all-gather.2
where the time goes:
time: 219 us; the launch traced here: 218 us
  waiting for transfers between devices  115 us (53%)
  starting transfers between devices  42.2 us (19%)
  between operations  15.2 us (7%)
  blocking collectives  14.6 us (7%)
  local copies, waits for them, and re-layouts  12.3 us (6%)
  other arithmetic  10.4 us (5%)
  matrix products  7.78 us (4%)
    all_gather x1, waiting for transfers between devices, over_pieces(): tiles = lax.all_gather(value, axis).astype(jnp.float32)  42.1 us
    all_to_all x1, waiting for transfers between devices, per_device(): lax.all_to_all(outgoing, 'ep', split_axis=0, concat_axis=0, tiled=True)  26 us
    all_to_all x2, waiting for transfers between devices, copy_for_each(): return lax.all_to_all(copies, axis, split_axis=0, concat_axis=0, tiled=True)  17.8 us
    all_to_all x1, blocking collectives, per_device(): lax.all_to_all(head_latent, 'tp', split_axis=1, concat_axis=0, tiled=True)  14.6 us
    all_to_all x2, starting transfers between devices, copy_for_each(): return lax.all_to_all(copies, axis, split_axis=0, concat_axis=0, tiled=True)  13.6 us
    all_to_all x1, starting transfers between devices, per_device(): lax.all_to_all(outgoing, 'ep', split_axis=0, concat_axis=0, tiled=True)  9.9 us
    all_to_all x1, waiting for transfers between devices, expert_tail(): lax.all_to_all(down_mat, 'tp', split_axis=1, concat_axis=0, tiled=True)  9.3 us
    all_to_all x1, waiting for transfers between devices, expert_tail(): return lax.all_to_all(summed, 'ep', split_axis=0, concat_axis=0, tiled=True)  8.16 us
  transfers between devices with their start and end apart: 8, of which 8 were waited for; matrix products, arithmetic and copies ran while one was open for 4% of the time, Pallas kernels for 0%

commit v1 on v0

v1 whole, which is shorter than its diff:
```python
import functools

import jax
import jax.numpy as jnp
from jax import lax
from jax.experimental import pallas as pl
from jax.experimental.pallas import tpu as pltpu
from jax.sharding import PartitionSpec as P

MESH = pl.DeviceIdType.MESH
F32 = jnp.float32
BF16 = jnp.bfloat16
HIGHEST = lax.Precision.HIGHEST

QK_NOPE = 128
QK_ROPE = 64
norm_floor = 1e-06
rope_base = 10000.0
masked_score = -1e30

LAT_AT, KEY_AT, ROT_AT, KEY_ROT_AT, MESSAGE = 0, 256, 512, 640, 768


def dot(a, b, precision=None):
    return lax.dot_general(
        a, b, (((1,), (0,)), ((), ())), preferred_element_type=F32, precision=precision
    )


def dot_t(a, b, precision=None):
    return lax.dot_general(
        a, b, (((1,), (1,)), ((), ())), preferred_element_type=F32, precision=precision
    )


def swap_halves(x):
    half = x.shape[-1] // 2
    return jnp.concatenate([x[:, half:], x[:, :half]], axis=1)


def iota(shape, dim):
    return lax.broadcasted_iota(jnp.int32, shape, dim)


def kernel(
    n_tp,
    n_ep,
    tokens,
    lengths,
    latent_cache,
    rope_cache,
    gains,
    turns,
    query_weight,
    query_rot_weight,
    latent_weight,
    key_rot_weight,
    absorb_weight,
    value_weight,
    output_weight,
    gate_weight,
    up_weight,
    down_weight,
    expert_ids,
    route_weights,
    out,
    new_latent,
    new_rope,
    lat_v,
    rope_v,
    qw_v,
    qrw_v,
    lw_v,
    krw_v,
    abs_v,
    val_v,
    ow_v,
    gate_v,
    up_v,
    down_v,
    tok_f,
    normed_b,
    msg_f,
    lat_f,
    route_f,
    tok_in,
    qry_out,
    qry_in,
    att_out,
    att_in,
    mix_out,
    mix_in,
    sum_in,
    dis_out,
    dis_in,
    part_out,
    part_in,
    hid_in,
    ret_out,
    ret_in,
    gate_in,
    up_in,
    down_in,
    local_sems,
    send_sems,
    recv_sems,
):
    me = lax.axis_index("tp")
    group = lax.axis_index("ep")
    rows = tok_f.shape[0]
    own = rows // n_tp
    width = tok_f.shape[1]
    cols = width // n_tp
    slots = dis_out.shape[1]
    ff_dev = gate_v.shape[0]
    latent = abs_v.shape[1]
    my_cols = pl.ds(pl.multiple_of(me * cols, cols), cols)

    def load(index, src, dst):
        copy = pltpu.make_async_copy(src, dst, local_sems.at[index])
        copy.start()
        return copy

    tok_copy = load(0, tokens, tok_in.at[me])
    qw_copy = load(1, query_weight, qw_v)
    qrw_copy = load(2, query_rot_weight, qrw_v)
    lw_copy = load(3, latent_weight, lw_v)
    krw_copy = load(4, key_rot_weight, krw_v)
    abs_copy = load(5, absorb_weight.at[0], abs_v)
    gate_copy = load(6, gate_weight.at[0], gate_v)
    up_copy = load(7, up_weight.at[0], up_v)
    lat_copy = load(8, latent_cache, lat_v)
    rope_copy = load(9, rope_cache, rope_v)
    val_copy = load(10, value_weight.at[0], val_v)
    ow_copy = load(11, output_weight, ow_v)
    down_copy = load(12, down_weight.at[0], down_v)

    barrier = pltpu.get_barrier_semaphore()

    def greet_tp(d, _):
        pl.semaphore_signal(
            barrier, inc=1, device_id={"tp": lax.rem(me + d, n_tp)}, device_id_type=MESH
        )
        return 0

    def greet_ep(d, _):
        pl.semaphore_signal(
            barrier, inc=1, device_id={"ep": lax.rem(group + d, n_ep)}, device_id_type=MESH
        )
        return 0

    lax.fori_loop(1, n_ep, greet_ep, 0)
    lax.fori_loop(1, n_tp, greet_tp, 0)
    pl.semaphore_wait(barrier, n_tp - 1 + n_ep - 1)

    order = sorted(range(1, n_tp), key=lambda d: -min(d, n_tp - d))

    def send(src, dst, stage, device):
        pltpu.make_async_remote_copy(
            src_ref=src,
            dst_ref=dst,
            send_sem=send_sems.at[stage],
            recv_sem=recv_sems.at[stage],
            device_id=device,
            device_id_type=MESH,
        ).start()

    def send_tp(stage, src_of, dst, before=None):
        for d in order:
            peer = lax.rem(me + d, n_tp)
            send(src_of(peer), dst, stage, {"tp": peer})

    def send_ep(stage, src_of, dst):
        def step(d, _):
            peer = lax.rem(group + d, n_ep)
            send(src_of(peer), dst, stage, {"ep": peer})
            return 0

        lax.fori_loop(1, n_ep, step, 0)

    def arrived(stage, buffer):
        some = buffer.at[pl.ds(0, buffer.shape[0] - 1)]
        pltpu.make_async_copy(some, some, recv_sems.at[stage]).wait()

    def sent(stage, buffer):
        some = buffer.at[pl.ds(0, buffer.shape[0] - 1)]
        pltpu.make_async_copy(some, some, send_sems.at[stage]).wait()

    tok_copy.wait()
    send_tp(0, lambda peer: tok_in.at[me], tok_in.at[me])

    square = (rows, rows)
    eye = (iota(square, 0) == iota(square, 1)).astype(F32)
    ahead_row = iota(square, 0) < iota(square, 1)
    ahead_col = iota(square, 1) < iota(square, 0)
    ids = expert_ids[...].astype(F32)
    weights_row = route_weights[...]
    id_rows = [ids[k : k + 1, :] for k in range(2)]
    id_cols = [jnp.sum(eye * r, axis=1, keepdims=True) for r in id_rows]
    weight_cols = [
        jnp.sum(eye * weights_row[k : k + 1, :], axis=1, keepdims=True) for k in range(2)
    ]

    def same(j, k):
        return id_cols[j] == id_rows[k]

    def count(mask, axis):
        return jnp.sum(jnp.where(mask, 1.0, 0.0), axis=axis, keepdims=True)

    rank_row0 = count(same(0, 0) & ahead_row, 0)
    rank_row1 = count(same(0, 1), 0) + count(same(1, 1) & ahead_row, 0)
    rank_col0 = count(same(0, 0) & ahead_col, 1)
    rank_col1 = count(same(1, 0), 1) + count(same(1, 1) & ahead_col, 1)
    target_rows = [id_rows[0] * slots + rank_row0, id_rows[1] * slots + rank_row1]
    target_cols = [id_cols[0] * slots + rank_col0, id_cols[1] * slots + rank_col1]
    all_slots = n_ep * slots
    down_iota = iota((all_slots, rows), 0).astype(F32)
    across_iota = iota((rows, all_slots), 1).astype(F32)
    dispatch = (
        jnp.where(down_iota == target_rows[0], 1.0, 0.0)
        + jnp.where(down_iota == target_rows[1], 1.0, 0.0)
    ).astype(BF16)
    combine = jnp.where(across_iota == target_cols[0], weight_cols[0], 0.0) + jnp.where(
        across_iota == target_cols[1], weight_cols[1], 0.0
    )

    arrived(0, tok_in)
    for t in range(n_tp):
        tok_f[own * t : own * (t + 1), :] = tok_in[t].astype(F32)
    chunk = 512
    square_sum = jnp.zeros((rows, 1), F32)
    for c in range(0, width, chunk):
        x = tok_f[:, c : c + chunk]
        square_sum = square_sum + jnp.sum(x * x, axis=1, keepdims=True)
    factor = lax.rsqrt(square_sum / width + norm_floor)
    for c in range(0, width, chunk):
        x = tok_f[:, c : c + chunk]
        normed_b[:, c : c + chunk] = (x * factor * gains[0:1, c : c + chunk]).astype(BF16)

    cosine, sine = turns[0], turns[1]
    qw_copy.wait()
    q_nope = dot(normed_b[...], qw_v[...]).astype(BF16)
    abs_copy.wait()
    msg_f[:, LAT_AT : LAT_AT + latent] = dot(q_nope, abs_v[...])
    qrw_copy.wait()
    q_rot = dot_t(normed_b[...], qrw_v[...])
    msg_f[:, ROT_AT : ROT_AT + QK_ROPE] = q_rot * cosine + swap_halves(q_rot) * sine
    slice_rows = normed_b[:, my_cols]
    lw_copy.wait()
    msg_f[:, KEY_AT : KEY_AT + latent] = dot(slice_rows, lw_v[...])
    krw_copy.wait()
    msg_f[:, KEY_ROT_AT : KEY_ROT_AT + QK_ROPE] = dot_t(slice_rows, krw_v[...])
    for t in range(n_tp):
        qry_out[t] = msg_f[own * t : own * (t + 1), :].astype(BF16)

    send_tp(1, lambda peer: qry_out.at[peer], qry_in.at[me])
    qry_in[me] = qry_out[me]
    gate_copy.wait()

    def piece(ref, peer):
        return ref.at[:, pl.ds(pl.multiple_of(peer * cols, cols), cols)]

    send_tp(2, lambda peer: piece(gate_v, peer), gate_in.at[me])
    gate_in[me] = gate_v[:, my_cols]

    own_rows = (iota((8, rows), 1) == own * me + iota((8, rows), 0)).astype(F32)
    own_cosine = dot(own_rows, cosine, HIGHEST)[:own]
    own_sine = dot(own_rows, sine, HIGHEST)[:own]
    lat_copy.wait()
    rope_copy.wait()

    arrived(1, qry_in)
    key_sum = jnp.zeros((own, MESSAGE), F32)
    for h in range(n_tp):
        part = qry_in[h].astype(F32)
        key_sum = key_sum + part
        msg_f[own * h : own * (h + 1), :] = part
    key_raw = key_sum[:, KEY_AT : KEY_AT + latent]
    key_factor = lax.rsqrt(jnp.mean(key_raw * key_raw, axis=1, keepdims=True) + norm_floor)
    own_lat = (key_raw * key_factor * gains[3:4, :latent]).astype(BF16)
    rope_raw = key_sum[:, KEY_ROT_AT : KEY_ROT_AT + QK_ROPE]
    own_rot = (rope_raw * own_cosine + swap_halves(rope_raw) * own_sine).astype(BF16)
    new_latent[...] = own_lat
    new_rope[...] = own_rot
    own_lat = own_lat.astype(F32)
    own_rot = own_rot.astype(F32)

    scale = (QK_NOPE + QK_ROPE) ** (-0.5)
    queries = msg_f[:, LAT_AT : LAT_AT + latent]
    rotated = msg_f[:, ROT_AT : ROT_AT + QK_ROPE]
    queries_b = queries.astype(BF16)
    rotated_b = rotated.astype(BF16)
    context = lat_v.shape[1]
    row_col = iota((rows, 1), 0)
    first = lax.rem(row_col, own) == 0

    def of_row(a, b):
        return jnp.where(first, a, b)

    scores = of_row(
        dot_t(queries_b, lat_v[0]) + dot(rotated_b, rope_v[0]),
        dot_t(queries_b, lat_v[1]) + dot(rotated_b, rope_v[1]),
    )
    row_len = of_row(lengths[own * me], lengths[own * me + 1])
    valid = iota((rows, context), 1) < row_len
    scores = jnp.where(valid, scores * scale, masked_score)
    lat_rows = of_row(own_lat[0:1], own_lat[1:2])
    rot_rows = of_row(own_rot[0:1], own_rot[1:2])
    own_score = (
        jnp.sum(queries * lat_rows, axis=1, keepdims=True)
        + jnp.sum(rotated * rot_rows, axis=1, keepdims=True)
    ) * scale
    top = jnp.maximum(jnp.max(scores, axis=1, keepdims=True), own_score)
    weights = jnp.where(valid, jnp.exp(scores - top), 0.0)
    own_weight = jnp.exp(own_score - top)
    total = jnp.sum(weights, axis=1, keepdims=True) + own_weight
    summed = (
        dot(jnp.where(first, weights, 0.0).astype(BF16), lat_v[0])
        + dot(jnp.where(first, 0.0, weights).astype(BF16), lat_v[1])
        + own_weight.astype(BF16).astype(F32) * lat_rows
    )
    lat_f[...] = summed / total
    for h in range(n_tp):
        att_out[h] = lat_f[own * h : own * (h + 1), :].astype(BF16)

    send_tp(3, lambda peer: att_out.at[peer], att_in.at[me])
    att_in[me] = att_out[me]
    up_copy.wait()
    send_tp(4, lambda peer: piece(up_v, peer), up_in.at[me])
    up_in[me] = up_v[:, my_cols]
    val_copy.wait()
    ow_copy.wait()

    arrived(3, att_in)
    for t in range(n_tp):
        lat_f[own * t : own * (t + 1), :] = att_in[t].astype(F32)
    head_values = dot(lat_f[...].astype(BF16), val_v[...]).astype(BF16)

    for d in order + [0]:
        peer = lax.rem(me + d, n_tp)
        share = dot(
            head_values, ow_v[:, pl.ds(pl.multiple_of(peer * cols, cols), cols)]
        ).astype(BF16)
        if d:
            mix_out[peer] = share
            send(mix_out.at[peer], mix_in.at[me], 5, {"tp": peer})
        else:
            mix_in[me] = share

    tok_cols = tok_f[:, my_cols]
    mix_gain = gains[1:2, my_cols]
    expert_gain = gains[2:3, my_cols]

    arrived(5, mix_in)
    mixed = mix_in[0].astype(F32)
    for t in range(1, n_tp):
        mixed = mixed + mix_in[t].astype(F32)
    mixed = mixed.astype(BF16).astype(F32)
    scaled = mixed * mix_gain

    def as_row(col):
        return jnp.sum(eye * col, axis=0, keepdims=True)

    def as_col(row):
        return jnp.sum(eye * row, axis=1, keepdims=True)

    def row_sum(value):
        return as_row(jnp.sum(value, axis=1, keepdims=True))

    sums = jnp.concatenate(
        [
            row_sum(mixed * mixed),
            row_sum(tok_cols * scaled),
            row_sum(scaled * scaled),
            jnp.zeros((1, rows), F32),
        ],
        axis=1,
    )
    sum_in[me] = sums
    send_tp(6, lambda peer: sum_in.at[me], sum_in.at[me])
    arrived(6, sum_in)
    sums = sum_in[0]
    for t in range(1, n_tp):
        sums = sums + sum_in[t]
    mix_square = as_col(sums[:, 0:rows])
    cross = as_col(sums[:, rows : 2 * rows])
    scaled_square = as_col(sums[:, 2 * rows : 3 * rows])
    mix_factor = lax.rsqrt(mix_square / width + norm_floor)
    resid = (tok_cols + scaled * mix_factor).astype(BF16).astype(F32)
    resid_square = square_sum + mix_factor * (2.0 * cross + mix_factor * scaled_square)
    resid_factor = lax.rsqrt(jnp.maximum(resid_square, 0.0) / width + norm_floor)
    expert_in = (resid * resid_factor * expert_gain).astype(BF16)

    route_f[...] = dot(dispatch, expert_in)
    for e in range(n_ep):
        dis_out[e] = route_f[slots * e : slots * (e + 1), :].astype(BF16)
    send_ep(7, lambda peer: dis_out.at[peer], dis_in.at[group])
    dis_in[group] = dis_out[group]
    down_copy.wait()
    send_tp(8, lambda peer: piece(down_v, peer), down_in.at[me])
    down_in[me] = down_v[:, my_cols]

    arrived(2, gate_in)
    arrived(4, up_in)
    arrived(7, dis_in)
    for g in range(n_ep):
        route_f[slots * g : slots * (g + 1), :] = dis_in[g].astype(F32)
    received = route_f[...].astype(BF16)
    ff = n_tp * ff_dev
    out_rows = all_slots // n_tp
    for n, source in enumerate((gate_in, up_in)):
        part = dot_t(received, source[...].reshape(ff, cols))
        part_out[:, :, n * ff : (n + 1) * ff] = part.reshape(n_tp, out_rows, ff).astype(BF16)

    send_tp(9, lambda peer: part_out.at[peer], part_in.at[me])
    part_in[me] = part_out[me]
    arrived(9, part_in)
    both = part_in[0].astype(F32)
    for t in range(1, n_tp):
        both = both + part_in[t].astype(F32)
    gate, upward = both[:, :ff], both[:, ff:]
    hid_in[me] = (gate / (1.0 + jnp.exp(-gate)) * upward).astype(BF16)

    send_tp(10, lambda peer: hid_in.at[me], hid_in.at[me])
    arrived(8, down_in)
    arrived(10, hid_in)
    hidden = hid_in[...].astype(F32).reshape(all_slots, ff).astype(BF16)
    route_f[...] = dot(hidden, down_in[...].reshape(ff, cols))
    for g in range(n_ep):
        ret_out[g] = route_f[slots * g : slots * (g + 1), :].astype(BF16)

    send_ep(11, lambda peer: ret_out.at[peer], ret_in.at[group])
    ret_in[group] = ret_out[group]
    arrived(11, ret_in)
    for e in range(n_ep):
        route_f[slots * e : slots * (e + 1), :] = ret_in[e].astype(F32)
    out[...] = (resid + dot(combine, route_f[...], HIGHEST)).astype(BF16)

    for stage, buffer in (
        (0, tok_in),
        (1, qry_in),
        (2, gate_in),
        (3, att_in),
        (4, up_in),
        (5, mix_in),
        (6, sum_in),
        (7, dis_in),
        (8, down_in),
        (9, part_in),
        (10, hid_in),
        (11, ret_in),
    ):
        sent(stage, buffer)


def per_device(
    tokens,
    lengths,
    latent_cache,
    rope_cache,
    attn_gain,
    query_weight,
    query_rot_weight,
    latent_weight,
    key_rot_weight,
    latent_gain,
    absorb_weight,
    value_weight,
    output_weight,
    mix_gain,
    expert_gain,
    gate_weight,
    up_weight,
    down_weight,
    expert_ids,
    route_weights,
):
    n_tp, n_ep = lax.axis_size("tp"), lax.axis_size("ep")
    own, width = tokens.shape
    rows = own * n_tp
    cols = width // n_tp
    latent = latent_weight.shape[1]
    context = latent_cache.shape[1]
    ff_dev = gate_weight.shape[2]
    ff = ff_dev * n_tp
    slots = 2 * rows * expert_ids.shape[1] // n_ep
    all_slots = n_ep * slots
    out_rows = all_slots // n_tp

    half = QK_ROPE // 2
    freqs = rope_base ** (-jnp.arange(half, dtype=F32) / half)
    angles = lengths.astype(F32)[:, None] * freqs
    cosine, sine = jnp.cos(angles), jnp.sin(angles)
    turns = jnp.stack(
        [jnp.concatenate([cosine, cosine], 1), jnp.concatenate([-sine, sine], 1)]
    )
    gains = jnp.stack(
        [attn_gain, mix_gain, expert_gain, jnp.pad(latent_gain, (0, width - latent))]
    ).astype(F32)

    operands = (
        tokens,
        lengths,
        latent_cache,
        jnp.swapaxes(rope_cache, 1, 2),
        gains,
        turns,
        query_weight,
        query_rot_weight.T,
        latent_weight,
        key_rot_weight.T,
        absorb_weight,
        value_weight,
        output_weight,
        jnp.swapaxes(gate_weight, 1, 2),
        jnp.swapaxes(up_weight, 1, 2),
        down_weight,
        expert_ids.T,
        route_weights.T,
    )
    spaces = {1: pltpu.SMEM, 4: pltpu.VMEM, 5: pltpu.VMEM, 16: pltpu.VMEM, 17: pltpu.VMEM}
    vmem = pltpu.VMEM
    return pl.pallas_call(
        functools.partial(kernel, n_tp, n_ep),
        out_shape=(
            jax.ShapeDtypeStruct((rows, cols), BF16),
            jax.ShapeDtypeStruct((own, latent), BF16),
            jax.ShapeDtypeStruct((own, QK_ROPE), BF16),
        ),
        in_specs=[
            pl.BlockSpec(memory_space=spaces.get(i, pl.ANY)) for i in range(len(operands))
        ],
        out_specs=[pl.BlockSpec(memory_space=vmem)] * 3,
        scratch_shapes=[
            vmem(latent_cache.shape, BF16),
            vmem((own, QK_ROPE, context), BF16),
            vmem(query_weight.shape, BF16),
            vmem((QK_ROPE, width), BF16),
            vmem(latent_weight.shape, BF16),
            vmem((QK_ROPE, cols), BF16),
            vmem(absorb_weight.shape[1:], BF16),
            vmem(value_weight.shape[1:], BF16),
            vmem(output_weight.shape, BF16),
            vmem((ff_dev, width), BF16),
            vmem((ff_dev, width), BF16),
            vmem((ff_dev, width), BF16),
            vmem((rows, width), F32),
            vmem((rows, width), BF16),
            vmem((rows, MESSAGE), F32),
            vmem((rows, latent), F32),
            vmem((all_slots, cols), F32),
            vmem((n_tp, own, width), BF16),
            vmem((n_tp, own, MESSAGE), BF16),
            vmem((n_tp, own, MESSAGE), BF16),
            vmem((n_tp, own, latent), BF16),
            vmem((n_tp, own, latent), BF16),
            vmem((n_tp, rows, cols), BF16),
            vmem((n_tp, rows, cols), BF16),
            vmem((n_tp, 1, 4 * rows), F32),
            vmem((n_ep, slots, cols), BF16),
            vmem((n_ep, slots, cols), BF16),
            vmem((n_tp, out_rows, 2 * ff), BF16),
            vmem((n_tp, out_rows, 2 * ff), BF16),
            vmem((n_tp, out_rows, ff), BF16),
            vmem((n_ep, slots, cols), BF16),
            vmem((n_ep, slots, cols), BF16),
            vmem((n_tp, ff_dev, cols), BF16),
            vmem((n_tp, ff_dev, cols), BF16),
            vmem((n_tp, ff_dev, cols), BF16),
            pltpu.SemaphoreType.DMA((13,)),
            pltpu.SemaphoreType.DMA((12,)),
            pltpu.SemaphoreType.DMA((12,)),
        ],
        compiler_params=pltpu.CompilerParams(
            collective_id=0, has_side_effects=True, vmem_limit_bytes=48 * 1024 * 1024
        ),
    )(*operands)


def solution(mesh):
    placed = (
        P(("ep", "tp"), None),
        P("ep"),
        P(("ep", "tp"), None, None),
        P(("ep", "tp"), None, None),
        P(),
        P(None, "tp"),
        P(None, "tp"),
        P("tp", None),
        P("tp", None),
        P(),
        P("tp", None, None),
        P("tp", None, None),
        P("tp", None),
        P(),
        P(),
        P("ep", None, "tp"),
        P("ep", None, "tp"),
        P("ep", "tp", None),
        P("ep", None),
        P("ep", None),
    )
    return jax.shard_map(
        per_device,
        mesh=mesh,
        in_specs=placed,
        out_specs=(P("ep", "tp"), P(("ep", "tp"), None), P(("ep", "tp"), None)),
        check_vma=False,
    )
```

time: 219 us -> 95.2 us (0.43)
  waiting for transfers between devices: 115 us -> 0 us
  Pallas kernels: 0 us -> 77.7 us
  starting transfers between devices: 42.2 us -> 0 us
  blocking collectives: 14.6 us -> 0 us
  between operations: 15.2 us -> 0.74 us
  other arithmetic: 10.4 us -> 1.02 us
  matrix products: 7.78 us -> 0 us
  local copies, waits for them, and re-layouts: 12.3 us -> 15.1 us
    pallas_call x0 -> x1, Pallas kernels: none -> 77.7 us  [per_device(): pl.pallas_call(functools.partial(kernel, n_tp, n_ep), out_shape=(jax.Shap...]
    all_to_all x7 -> x0, waiting for transfers between devices: 73.1 us -> none  [the longest x1 26 us: per_device(): lax.all_to_all(outgoing, 'ep', split_axis=0, concat_axis=0, tiled=True)]
    all_gather x1 -> x0, waiting for transfers between devices: 42.1 us -> none  [over_pieces(): tiles = lax.all_gather(value, axis).astype(jnp.float32)]
    all_to_all x7 -> x0, starting transfers between devices: 42.1 us -> none  [the longest x2 13.6 us: copy_for_each(): return lax.all_to_all(copies, axis, split_axis=0, concat_axis=0, tiled=True)]
    all_to_all x1 -> x0, blocking collectives: 14.6 us -> none  [per_device(): lax.all_to_all(head_latent, 'tp', split_axis=1, concat_axis=0, tiled=True)]
    unnamed x38 -> x35, local copies, waits for them, and re-layouts: 2.89 us -> 12.3 us
    dot_general x13 -> x0, matrix products: 7.78 us -> none  [the longest x1 1.61 us: per_device(): jnp.einsum('thn,hnl->thl', q_nope, absorb_weight, preferred_element_type=...]
    reduce_sum x11 -> x0, other arithmetic: 4.99 us -> none  [the longest x1 2.98 us: over_pieces(): return tiles.sum(axis=0)]
  transfers between devices with their start and end apart: 8 -> 0, of which waited for: 8 -> 0; matrix products, arithmetic and copies ran while one was open for 4% -> 0% of each run, Pallas kernels for 0% -> 0%
where the time goes in v1:
time: 95.2 us; the launch traced here: 94.5 us
  Pallas kernels  77.7 us (82%)
  local copies, waits for them, and re-layouts  15.1 us (16%)
  other arithmetic  1.02 us (1%)
    pallas_call x1, Pallas kernels, per_device(): pl.pallas_call(functools.partial(kernel, n_tp, n_ep), out_shape=(jax.Shap...  77.7 us
    unnamed x35, local copies, waits for them, and re-layouts  12.3 us
    another operation x4, local copies, waits for them, and re-layouts, per_device(): jnp.stack([attn_gain, mix_gain, expert_gain, jnp.pad(latent_gain, (0, wid...  2.14 us

profile of v1, /device:TPU:1, one launch (start us, length us, event | category | flops | bytes accessed | tf_op | source)
XLA Modules:
  0.0 94.5 jit_solution(11715538049864571782)
XLA Ops:
  0.6 0.0 copy-start.4
  0.6 0.7 convert_element_type.9
  1.4 0.7 pad.4
  2.0 0.7 stack.24
  2.7 0.7 stack.25
  3.5 0.7 stack.26
  4.2 0.1 maximum_convert_fusion.gains
  4.3 0.0 copy-start.8
  4.3 0.1 multiply_cosine_fusion
  4.4 0.0 copy-start.9
  4.4 0.1 maximum_bitcast_fusion
  4.5 0.0 copy-start.15
  4.5 0.0 copy-done.4
  4.6 0.6 copy-done.8
  5.2 0.1 copy-done.9
  5.3 0.0 copy-done.13
  5.3 0.0 copy-done.14
  5.3 0.0 copy-done.15
  5.3 1.2 %copy-done = bf16[2,1024,256]{2,1,0:T(8,128)(2,1)S(1)} copy-done((bf16[2,1024,256]{2,1,0:T(8,128)(2,1)S(1)}, bf16[2,1024,256]{2,1,0:T(8,128)(2,1)}, u32[]{:S(2)}) %copy-start) | copy-done | bytes 1048600
  6.5 1.2 %copy-done.1 = bf16[4096,128]{1,0:T(8,128)(2,1)S(1)} copy-done((bf16[4096,128]{1,0:T(8,128)(2,1)S(1)}, bf16[4096,128]{1,0:T(8,128)(2,1)}, u32[]{:S(2)}) %copy-start.1) | copy-done | bytes 1048600
  7.7 1.2 %copy-done.2 = bf16[128,4096]{1,0:T(8,128)(2,1)S(1)} copy-done((bf16[128,4096]{1,0:T(8,128)(2,1)S(1)}, bf16[128,4096]{1,0:T(8,128)(2,1)}, u32[]{:S(2)}) %copy-start.2) | copy-done | bytes 1048600
  9.0 1.0 %copy-done.3 = bf16[4096,64]{0,1:T(8,128)(2,1)S(1)} copy-done((bf16[4096,64]{0,1:T(8,128)(2,1)S(1)}, bf16[4096,64]{0,1:T(8,128)(2,1)}, u32[]{:S(2)}) %copy-start.3) | copy-done | bytes 524312
  10.0 0.9 %copy-done.5 = bf16[1,4096,32]{1,2,0:T(8,128)(2,1)S(1)} copy-done((bf16[1,4096,32]{1,2,0:T(8,128)(2,1)S(1)}, bf16[1,4096,32]{1,2,0:T(8,128)(2,1)}, u32[]{:S(2)}) %copy-start.5) | copy-done | bytes 262168
  11.0 0.9 %copy-done.6 = bf16[1,4096,32]{1,2,0:T(8,128)(2,1)S(1)} copy-done((bf16[1,4096,32]{1,2,0:T(8,128)(2,1)S(1)}, bf16[1,4096,32]{1,2,0:T(8,128)(2,1)}, u32[]{:S(2)}) %copy-start.6) | copy-done | bytes 262168
  11.9 0.9 %copy-done.7 = bf16[1,32,4096]{2,1,0:T(8,128)(2,1)S(1)} copy-done((bf16[1,32,4096]{2,1,0:T(8,128)(2,1)S(1)}, bf16[1,32,4096]{2,1,0:T(8,128)(2,1)}, u32[]{:S(2)}) %copy-start.7) | copy-done | bytes 262168
  12.9 0.8 copy-done.10
  13.7 0.8 copy-done.11
  14.5 0.7 copy-done.12
  15.2 77.7 %shard_map.211 = (bf16[32,256]{1,0:T(8,128)(2,1)S(1)}, bf16[2,256]{1,0:T(2,128)(2,1)S(1)}, bf16[2,64]{1,0:T(2,128)(2,1)S(1)}) custom-call(bf16[2,4096]{1,0:T(2,128)(2,1)S(1)} %copy-done.12, s32[32]{0:T(128)S(1)} %copy-done.15, bf16[2,1024,256]{2,1,0:T(8,128)(2,1)S(1)} %copy-done, bf16[2,64,1024]{2,1,0:T(8,128)(2,1)S(1)} %bitcast.12, ...), custom_call_target="tpu_custom_call" | custom-call | tf_op jit(solution)/shard_map/pallas_call | solution.py:523
  92.8 0.6 copy.26
  93.5 0.6 copy.27
  94.0 0.5 copy.28
  (15 shorter events, 0.0 us)
Async XLA Ops:
  0.6 3.9 %copy-start.4 = (bf16[2,1024,64]{1,2,0:T(8,128)(2,1)S(1)}, bf16[2,1024,64]{1,2,0:T(8,128)(2,1)}, u32[]{:S(2)}) copy-start(bf16[2,1024,64]{1,2,0:T(8,128)(2,1)} %param.23) | copy-start | bytes 786436
  4.3 0.9 copy-start.8
  4.4 0.9 copy-start.9
  4.5 0.8 copy-start.13
  4.5 0.8 copy-start.14
  4.5 0.8 copy-start.15
  5.3 1.2 %copy-start = (bf16[2,1024,256]{2,1,0:T(8,128)(2,1)S(1)}, bf16[2,1024,256]{2,1,0:T(8,128)(2,1)}, u32[]{:S(2)}) copy-start(bf16[2,1024,256]{2,1,0:T(8,128)(2,1)} %latent_cache.1) | copy-start | bytes 3145732
  6.5 1.2 %copy-start.1 = (bf16[4096,128]{1,0:T(8,128)(2,1)S(1)}, bf16[4096,128]{1,0:T(8,128)(2,1)}, u32[]{:S(2)}) copy-start(bf16[4096,128]{1,0:T(8,128)(2,1)} %query_weight.1) | copy-start | bytes 3145732
  7.7 1.2 %copy-start.2 = (bf16[128,4096]{1,0:T(8,128)(2,1)S(1)}, bf16[128,4096]{1,0:T(8,128)(2,1)}, u32[]{:S(2)}) copy-start(bf16[128,4096]{1,0:T(8,128)(2,1)} %output_weight.1) | copy-start | bytes 3145732
  9.0 1.0 %copy-start.3 = (bf16[4096,64]{0,1:T(8,128)(2,1)S(1)}, bf16[4096,64]{0,1:T(8,128)(2,1)}, u32[]{:S(2)}) copy-start(bf16[4096,64]{0,1:T(8,128)(2,1)} %param.26) | copy-start | bytes 1572868
  10.0 0.9 %copy-start.5 = (bf16[1,4096,32]{1,2,0:T(8,128)(2,1)S(1)}, bf16[1,4096,32]{1,2,0:T(8,128)(2,1)}, u32[]{:S(2)}) copy-start(bf16[1,4096,32]{1,2,0:T(8,128)(2,1)} %param.35) | copy-start | bytes 786436
  11.0 0.9 %copy-start.6 = (bf16[1,4096,32]{1,2,0:T(8,128)(2,1)S(1)}, bf16[1,4096,32]{1,2,0:T(8,128)(2,1)}, u32[]{:S(2)}) copy-start(bf16[1,4096,32]{1,2,0:T(8,128)(2,1)} %param.36) | copy-start | bytes 786436
  11.9 0.9 %copy-start.7 = (bf16[1,32,4096]{2,1,0:T(8,128)(2,1)S(1)}, bf16[1,32,4096]{2,1,0:T(8,128)(2,1)}, u32[]{:S(2)}) copy-start(bf16[1,32,4096]{2,1,0:T(8,128)(2,1)} %down_weight.1) | copy-start | bytes 786436
  12.9 0.8 copy-start.10
  13.7 0.8 copy-start.11
  14.5 0.7 copy-start.12

commit v2 on v1

--- a/solution.py
+++ b/solution.py
@@ -2,6 +2,7 @@
 
 import jax
 import jax.numpy as jnp
+import numpy as np
 from jax import lax
 from jax.experimental import pallas as pl
 from jax.experimental.pallas import tpu as pltpu
@@ -36,6 +37,14 @@
 def swap_halves(x):
     half = x.shape[-1] // 2
     return jnp.concatenate([x[:, half:], x[:, :half]], axis=1)
+
+
+def gain_row(ref, first, size):
+    return ref[pl.ds(first, size)].astype(F32).reshape(1, size)
+
+
+def cos_sin(x):
+    return jnp.cos(x), jnp.sin(x)
 
 
 def iota(shape, dim):
@@ -49,8 +58,10 @@
     lengths,
     latent_cache,
     rope_cache,
-    gains,
-    turns,
+    attn_gain,
+    mix_gain,
+    expert_gain,
+    latent_gain,
     query_weight,
     query_rot_weight,
     latent_weight,
@@ -66,6 +77,13 @@
     out,
     new_latent,
     new_rope,
+    len_v,
+    ids_v,
+    rw_v,
+    attn_v,
+    mixg_v,
+    expg_v,
+    latg_v,
     lat_v,
     rope_v,
     qw_v,
@@ -114,7 +132,8 @@
     slots = dis_out.shape[1]
     ff_dev = gate_v.shape[0]
     latent = abs_v.shape[1]
-    my_cols = pl.ds(pl.multiple_of(me * cols, cols), cols)
+    my_first = pl.multiple_of(me * cols, cols)
+    my_cols = pl.ds(my_first, cols)
 
     def load(index, src, dst):
         copy = pltpu.make_async_copy(src, dst, local_sems.at[index])
@@ -122,6 +141,15 @@
         return copy
 
     tok_copy = load(0, tokens, tok_in.at[me])
+    small = [
+        load(13, lengths, len_v),
+        load(14, expert_ids, ids_v),
+        load(15, route_weights, rw_v),
+        load(16, attn_gain, attn_v),
+        load(17, mix_gain, mixg_v),
+        load(18, expert_gain, expg_v),
+        load(19, latent_gain, latg_v),
+    ]
     qw_copy = load(1, query_weight, qw_v)
     qrw_copy = load(2, query_rot_weight, qrw_v)
     lw_copy = load(3, latent_weight, lw_v)
@@ -193,8 +221,10 @@
     eye = (iota(square, 0) == iota(square, 1)).astype(F32)
     ahead_row = iota(square, 0) < iota(square, 1)
     ahead_col = iota(square, 1) < iota(square, 0)
-    ids = expert_ids[...].astype(F32)
-    weights_row = route_weights[...]
+    for copy in small:
+        copy.wait()
+    ids = ids_v[...].astype(F32)
+    weights_row = rw_v[...]
     id_rows = [ids[k : k + 1, :] for k in range(2)]
     id_cols = [jnp.sum(eye * r, axis=1, keepdims=True) for r in id_rows]
     weight_cols = [
@@ -224,6 +254,20 @@
         across_iota == target_cols[1], weight_cols[1], 0.0
     )
 
+    half = QK_ROPE // 2
+    freqs = jnp.zeros((1, QK_ROPE), F32)
+    lane = lax.rem(iota((1, QK_ROPE), 1), half)
+    for i in range(half):
+        freqs = jnp.where(lane == i, float(np.float32(rope_base ** (-i / half))), freqs)
+    lengths_row = len_v[...].astype(F32)
+    lengths_col = jnp.sum(eye * lengths_row, axis=1, keepdims=True)
+    cosine, sine = cos_sin(lengths_col * freqs)
+    sine = jnp.where(iota((1, QK_ROPE), 1) < half, -sine, sine)
+    own_rows = (iota((8, rows), 1) == own * me + iota((8, rows), 0)).astype(F32)
+    own_cosine = dot(own_rows, cosine, HIGHEST)[:own]
+    own_sine = dot(own_rows, sine, HIGHEST)[:own]
+    own_lengths = jnp.sum(own_rows * lengths_row, axis=1, keepdims=True).astype(jnp.int32)
+
     arrived(0, tok_in)
     for t in range(n_tp):
         tok_f[own * t : own * (t + 1), :] = tok_in[t].astype(F32)
@@ -235,9 +279,8 @@
     factor = lax.rsqrt(square_sum / width + norm_floor)
     for c in range(0, width, chunk):
         x = tok_f[:, c : c + chunk]
-        normed_b[:, c : c + chunk] = (x * factor * gains[0:1, c : c + chunk]).astype(BF16)
-
-    cosine, sine = turns[0], turns[1]
+        normed_b[:, c : c + chunk] = (x * factor * gain_row(attn_v, c, chunk)).astype(BF16)
+
     qw_copy.wait()
     q_nope = dot(normed_b[...], qw_v[...]).astype(BF16)
     abs_copy.wait()
@@ -263,9 +306,6 @@
     send_tp(2, lambda peer: piece(gate_v, peer), gate_in.at[me])
     gate_in[me] = gate_v[:, my_cols]
 
-    own_rows = (iota((8, rows), 1) == own * me + iota((8, rows), 0)).astype(F32)
-    own_cosine = dot(own_rows, cosine, HIGHEST)[:own]
-    own_sine = dot(own_rows, sine, HIGHEST)[:own]
     lat_copy.wait()
     rope_copy.wait()
 
@@ -277,7 +317,7 @@
         msg_f[own * h : own * (h + 1), :] = part
     key_raw = key_sum[:, KEY_AT : KEY_AT + latent]
     key_factor = lax.rsqrt(jnp.mean(key_raw * key_raw, axis=1, keepdims=True) + norm_floor)
-    own_lat = (key_raw * key_factor * gains[3:4, :latent]).astype(BF16)
+    own_lat = (key_raw * key_factor * gain_row(latg_v, 0, latent)).astype(BF16)
     rope_raw = key_sum[:, KEY_ROT_AT : KEY_ROT_AT + QK_ROPE]
     own_rot = (rope_raw * own_cosine + swap_halves(rope_raw) * own_sine).astype(BF16)
     new_latent[...] = own_lat
@@ -301,7 +341,7 @@
         dot_t(queries_b, lat_v[0]) + dot(rotated_b, rope_v[0]),
         dot_t(queries_b, lat_v[1]) + dot(rotated_b, rope_v[1]),
     )
-    row_len = of_row(lengths[own * me], lengths[own * me + 1])
+    row_len = of_row(own_lengths[0:1], own_lengths[1:2])
     valid = iota((rows, context), 1) < row_len
     scores = jnp.where(valid, scores * scale, masked_score)
     lat_rows = of_row(own_lat[0:1], own_lat[1:2])
@@ -348,15 +388,15 @@
             mix_in[me] = share
 
     tok_cols = tok_f[:, my_cols]
-    mix_gain = gains[1:2, my_cols]
-    expert_gain = gains[2:3, my_cols]
+    my_mix_gain = gain_row(mixg_v, my_first, cols)
+    my_expert_gain = gain_row(expg_v, my_first, cols)
 
     arrived(5, mix_in)
     mixed = mix_in[0].astype(F32)
     for t in range(1, n_tp):
         mixed = mixed + mix_in[t].astype(F32)
     mixed = mixed.astype(BF16).astype(F32)
-    scaled = mixed * mix_gain
+    scaled = mixed * my_mix_gain
 
     def as_row(col):
         return jnp.sum(eye * col, axis=0, keepdims=True)
@@ -389,7 +429,7 @@
     resid = (tok_cols + scaled * mix_factor).astype(BF16).astype(F32)
     resid_square = square_sum + mix_factor * (2.0 * cross + mix_factor * scaled_square)
     resid_factor = lax.rsqrt(jnp.maximum(resid_square, 0.0) / width + norm_floor)
-    expert_in = (resid * resid_factor * expert_gain).astype(BF16)
+    expert_in = (resid * resid_factor * my_expert_gain).astype(BF16)
 
     route_f[...] = dot(dispatch, expert_in)
     for e in range(n_ep):
@@ -487,24 +527,15 @@
     all_slots = n_ep * slots
     out_rows = all_slots // n_tp
 
-    half = QK_ROPE // 2
-    freqs = rope_base ** (-jnp.arange(half, dtype=F32) / half)
-    angles = lengths.astype(F32)[:, None] * freqs
-    cosine, sine = jnp.cos(angles), jnp.sin(angles)
-    turns = jnp.stack(
-        [jnp.concatenate([cosine, cosine], 1), jnp.concatenate([-sine, sine], 1)]
-    )
-    gains = jnp.stack(
-        [attn_gain, mix_gain, expert_gain, jnp.pad(latent_gain, (0, width - latent))]
-    ).astype(F32)
-
     operands = (
         tokens,
-        lengths,
+        lengths.reshape(1, rows),
         latent_cache,
         jnp.swapaxes(rope_cache, 1, 2),
-        gains,
-        turns,
+        attn_gain,
+        mix_gain,
+        expert_gain,
+        latent_gain,
         query_weight,
         query_rot_weight.T,
         latent_weight,
@@ -518,7 +549,6 @@
         expert_ids.T,
         route_weights.T,
     )
-    spaces = {1: pltpu.SMEM, 4: pltpu.VMEM, 5: pltpu.VMEM, 16: pltpu.VMEM, 17: pltpu.VMEM}
     vmem = pltpu.VMEM
     return pl.pallas_call(
         functools.partial(kernel, n_tp, n_ep),
@@ -528,10 +558,17 @@
             jax.ShapeDtypeStruct((own, QK_ROPE), BF16),
         ),
         in_specs=[
-            pl.BlockSpec(memory_space=spaces.get(i, pl.ANY)) for i in range(len(operands))
+            pl.BlockSpec(memory_space=pl.ANY) for _ in operands
         ],
         out_specs=[pl.BlockSpec(memory_space=vmem)] * 3,
         scratch_shapes=[
+            vmem((1, rows), jnp.int32),
+            vmem(expert_ids.shape[::-1], jnp.int32),
+            vmem(route_weights.shape[::-1], F32),
+            vmem((width,), BF16),
+            vmem((width,), BF16),
+            vmem((width,), BF16),
+            vmem((latent,), BF16),
             vmem(latent_cache.shape, BF16),
             vmem((own, QK_ROPE, context), BF16),
             vmem(query_weight.shape, BF16),
@@ -567,12 +604,12 @@
             vmem((n_tp, ff_dev, cols), BF16),
             vmem((n_tp, ff_dev, cols), BF16),
             vmem((n_tp, ff_dev, cols), BF16),
-            pltpu.SemaphoreType.DMA((13,)),
+            pltpu.SemaphoreType.DMA((20,)),
             pltpu.SemaphoreType.DMA((12,)),
             pltpu.SemaphoreType.DMA((12,)),
         ],
         compiler_params=pltpu.CompilerParams(
-            collective_id=0, has_side_effects=True, vmem_limit_bytes=48 * 1024 * 1024
+            collective_id=0, has_side_effects=True, vmem_limit_bytes=67_043_328
         ),
     )(*operands)
 

time: 95.2 us -> 80.6 us (0.85)
  local copies, waits for them, and re-layouts: 15.1 us -> 2.45 us
  other arithmetic: 1.02 us -> 0 us
    unnamed x35 -> x7, local copies, waits for them, and re-layouts: 12.3 us -> 2.45 us
    another operation x4 -> x0, local copies, waits for them, and re-layouts: 2.14 us -> none  [per_device(): jnp.stack([attn_gain, mix_gain, expert_gain, jnp.pad(latent_gain, (0, wid...]
where the time goes in v2:
time: 80.6 us; the launch traced here: 80.4 us
  Pallas kernels  77.3 us (96%)
  local copies, waits for them, and re-layouts  2.45 us (3%)
    pallas_call x1, Pallas kernels, per_device(): pl.pallas_call(functools.partial(kernel, n_tp, n_ep), out_shape=(jax.Shap...  77.3 us
    unnamed x7, local copies, waits for them, and re-layouts  2.45 us

profile of v2, /device:TPU:1, one launch (start us, length us, event | category | flops | bytes accessed | tf_op | source)
XLA Modules:
  0.0 80.4 jit_solution(2257582687793251521)
XLA Ops:
  0.6 77.3 %shard_map.211 = (bf16[32,256]{1,0:T(8,128)(2,1)}, bf16[2,256]{1,0:T(2,128)(2,1)}, bf16[2,64]{1,0:T(2,128)(2,1)}) custom-call(bf16[2,4096]{1,0:T(2,128)(2,1)} %tokens.1, s32[1,32]{1,0:T(1,128)} %bitcast.15, bf16[2,1024,256]{2,1,0:T(8,128)(2,1)} %latent_cache.1, bf16[2,64,1024]{2,1,0:T(8,128)(2,1)} %bitcast.9, bf16[4096]{0:T(1024)(128)(2,1)} %attn_gain.1, ...), custom_call_target="tpu_custom_call" | custom-call | tf_op jit(solution)/shard_map/pallas_call | solution.py:553
  78.0 0.0 copy-start
  78.0 1.3 %copy.26 = bf16[32,256]{1,0:T(8,128)(2,1)} copy(bf16[32,256]{1,0:T(8,128)(2,1)} %get-tuple-element.6) | data formatting | bytes 32768
  79.3 0.0 copy-done
  79.3 0.0 copy-start.1
  79.3 0.6 copy.27
  79.9 0.0 copy-done.1
  79.9 0.5 copy.28
Async XLA Ops:
  78.0 1.3 %copy-start = (bf16[2,256]{1,0:T(2,128)(2,1)S(1)}, bf16[2,256]{1,0:T(2,128)(2,1)}, u32[]{:S(2)}) copy-start(bf16[2,256]{1,0:T(2,128)(2,1)} %get-tuple-element.7) | copy-start | bytes 3076
  79.3 0.6 copy-start.1

commit v3 on v2

--- a/solution.py
+++ b/solution.py
@@ -91,8 +91,8 @@
     lw_v,
     krw_v,
     abs_v,
-    val_v,
-    ow_v,
+    val_pair,
+    ow_pair,
     gate_v,
     up_v,
     down_v,
@@ -122,6 +122,7 @@
     local_sems,
     send_sems,
     recv_sems,
+    tok_sems,
 ):
     me = lax.axis_index("tp")
     group = lax.axis_index("ep")
@@ -134,6 +135,13 @@
     latent = abs_v.shape[1]
     my_first = pl.multiple_of(me * cols, cols)
     my_cols = pl.ds(my_first, cols)
+    n_chip = n_tp // 2
+    half_ep = n_ep // 2
+    chip = me // 2
+    core = lax.rem(me, 2)
+    sibling = me + 1 - 2 * core
+    side = lax.rem(group, 2)
+    at_home = side == core
 
     def load(index, src, dst):
         copy = pltpu.make_async_copy(src, dst, local_sems.at[index])
@@ -141,6 +149,31 @@
         return copy
 
     tok_copy = load(0, tokens, tok_in.at[me])
+
+    barrier = pltpu.get_barrier_semaphore()
+
+    def greet(device):
+        pl.semaphore_signal(barrier, inc=1, device_id=device, device_id_type=MESH)
+
+    for d in range(1, n_tp):
+        greet({"tp": lax.rem(me + d, n_tp)})
+
+    def greet_ep(d, _):
+        greet({"ep": lax.rem(group + d, n_ep), "tp": 2 * chip + side})
+        return 0
+
+    lax.fori_loop(1, n_ep, greet_ep, 0)
+
+    @pl.when(jnp.logical_not(at_home))
+    def _():
+        greet({"tp": sibling})
+
+    def greet_back(d, _):
+        greet({"ep": 2 * d + core, "tp": 2 * chip + 1 - side})
+        return 0
+
+    lax.fori_loop(0, half_ep, greet_back, 0)
+
     small = [
         load(13, lengths, len_v),
         load(14, expert_ids, ids_v),
@@ -159,63 +192,80 @@
     up_copy = load(7, up_weight.at[0], up_v)
     lat_copy = load(8, latent_cache, lat_v)
     rope_copy = load(9, rope_cache, rope_v)
-    val_copy = load(10, value_weight.at[0], val_v)
-    ow_copy = load(11, output_weight, ow_v)
+    val_copy = load(10, value_weight.at[0], val_pair.at[core])
+    value_dim = value_weight.shape[2]
+    head_rows = pl.ds(pl.multiple_of(core * value_dim, value_dim), value_dim)
+
+    def block(index):
+        return pl.ds(pl.multiple_of(index * cols, cols), cols)
+
+    for y in range(n_chip):
+        pltpu.make_async_copy(
+            output_weight.at[:, block(2 * y + core)],
+            ow_pair.at[y, head_rows],
+            local_sems.at[11],
+        ).start()
     down_copy = load(12, down_weight.at[0], down_v)
 
-    barrier = pltpu.get_barrier_semaphore()
-
-    def greet_tp(d, _):
-        pl.semaphore_signal(
-            barrier, inc=1, device_id={"tp": lax.rem(me + d, n_tp)}, device_id_type=MESH
-        )
-        return 0
-
-    def greet_ep(d, _):
-        pl.semaphore_signal(
-            barrier, inc=1, device_id={"ep": lax.rem(group + d, n_ep)}, device_id_type=MESH
-        )
-        return 0
-
-    lax.fori_loop(1, n_ep, greet_ep, 0)
-    lax.fori_loop(1, n_tp, greet_tp, 0)
-    pl.semaphore_wait(barrier, n_tp - 1 + n_ep - 1)
+    pl.semaphore_wait(
+        barrier, n_tp - 1 + n_ep + half_ep - jnp.where(at_home, 1, 0)
+    )
 
     order = sorted(range(1, n_tp), key=lambda d: -min(d, n_tp - d))
-
-    def send(src, dst, stage, device):
+    chip_order = sorted(range(1, n_chip), key=lambda d: -min(d, n_chip - d))
+
+    def send(src, dst, stage, device, recv_sem=None):
         pltpu.make_async_remote_copy(
             src_ref=src,
             dst_ref=dst,
             send_sem=send_sems.at[stage],
-            recv_sem=recv_sems.at[stage],
+            recv_sem=recv_sems.at[stage] if recv_sem is None else recv_sem,
             device_id=device,
             device_id_type=MESH,
         ).start()
 
-    def send_tp(stage, src_of, dst, before=None):
+    def send_tp(stage, src_of, dst):
         for d in order:
             peer = lax.rem(me + d, n_tp)
-            send(src_of(peer), dst, stage, {"tp": peer})
-
-    def send_ep(stage, src_of, dst):
-        def step(d, _):
-            peer = lax.rem(group + d, n_ep)
-            send(src_of(peer), dst, stage, {"ep": peer})
-            return 0
-
-        lax.fori_loop(1, n_ep, step, 0)
-
-    def arrived(stage, buffer):
-        some = buffer.at[pl.ds(0, buffer.shape[0] - 1)]
-        pltpu.make_async_copy(some, some, recv_sems.at[stage]).wait()
-
-    def sent(stage, buffer):
-        some = buffer.at[pl.ds(0, buffer.shape[0] - 1)]
-        pltpu.make_async_copy(some, some, send_sems.at[stage]).wait()
+            send(src_of(peer), dst(peer) if callable(dst) else dst, stage, {"tp": peer})
+
+    def send_chips(stage, src_of, dst):
+        for d in chip_order:
+            peer = lax.rem(chip + d, n_chip)
+            send(src_of(peer), dst, stage, {"tp": 2 * peer + core})
+
+    def wait_for(sem, buffer, count):
+        some = buffer.at[pl.ds(0, count)]
+        pltpu.make_async_copy(some, some, sem).wait()
+
+    def arrived(stage, buffer, count=None):
+        wait_for(recv_sems.at[stage], buffer, buffer.shape[0] - 1 if count is None else count)
+
+    def sent(stage, buffer, count=None):
+        wait_for(send_sems.at[stage], buffer, buffer.shape[0] - 1 if count is None else count)
+
+    def arrived_all(stage, buffer):
+        pltpu.make_async_copy(buffer, buffer, recv_sems.at[stage]).wait()
+
+    def sent_all(stage, buffer):
+        pltpu.make_async_copy(buffer, buffer, send_sems.at[stage]).wait()
+
+    def at_home_or_not(stage, buffer, sems):
+        count = buffer.shape[0]
+
+        @pl.when(at_home)
+        def _():
+            wait_for(sems.at[stage], buffer, count - 1)
+
+        @pl.when(jnp.logical_not(at_home))
+        def _():
+            wait_for(sems.at[stage], buffer, count)
 
     tok_copy.wait()
-    send_tp(0, lambda peer: tok_in.at[me], tok_in.at[me])
+    send(tok_in.at[me], tok_in.at[me], 0, {"tp": sibling}, recv_sems.at[12])
+    for d in chip_order:
+        peer = lax.rem(chip + d, n_chip)
+        send(tok_in.at[me], tok_in.at[me], 0, {"tp": 2 * peer + core}, tok_sems.at[chip])
 
     square = (rows, rows)
     eye = (iota(square, 0) == iota(square, 1)).astype(F32)
@@ -268,7 +318,12 @@
     own_sine = dot(own_rows, sine, HIGHEST)[:own]
     own_lengths = jnp.sum(own_rows * lengths_row, axis=1, keepdims=True).astype(jnp.int32)
 
-    arrived(0, tok_in)
+    for d in reversed(chip_order):
+        peer = lax.rem(chip + d, n_chip)
+        slot = tok_in.at[2 * peer + core]
+        pltpu.make_async_copy(slot, slot, tok_sems.at[peer]).wait()
+        send(slot, slot, 0, {"tp": sibling}, recv_sems.at[12])
+    arrived(12, tok_in, n_chip)
     for t in range(n_tp):
         tok_f[own * t : own * (t + 1), :] = tok_in[t].astype(F32)
     chunk = 512
@@ -298,13 +353,24 @@
 
     send_tp(1, lambda peer: qry_out.at[peer], qry_in.at[me])
     qry_in[me] = qry_out[me]
+    send(value_weight.at[0], val_pair.at[core], 16, {"tp": sibling})
+    for y in range(n_chip):
+        send(
+            output_weight.at[:, block(2 * y + 1 - core)],
+            ow_pair.at[y, head_rows],
+            17,
+            {"tp": sibling},
+        )
     gate_copy.wait()
 
     def piece(ref, peer):
         return ref.at[:, pl.ds(pl.multiple_of(peer * cols, cols), cols)]
 
-    send_tp(2, lambda peer: piece(gate_v, peer), gate_in.at[me])
-    gate_in[me] = gate_v[:, my_cols]
+    def half_of(ref):
+        return lambda peer: ref.at[lax.rem(peer, 2), me]
+
+    send_tp(2, lambda peer: piece(gate_v, peer), half_of(gate_in))
+    gate_in[core, me] = gate_v[:, my_cols]
 
     lat_copy.wait()
     rope_copy.wait()
@@ -360,40 +426,51 @@
         + own_weight.astype(BF16).astype(F32) * lat_rows
     )
     lat_f[...] = summed / total
-    for h in range(n_tp):
-        att_out[h] = lat_f[own * h : own * (h + 1), :].astype(BF16)
-
-    send_tp(3, lambda peer: att_out.at[peer], att_in.at[me])
-    att_in[me] = att_out[me]
+    for y in range(n_chip):
+        for c in range(2):
+            at = own * (2 * y + c)
+            att_out[y, :, c * latent : (c + 1) * latent] = lat_f[at : at + own, :].astype(BF16)
+
+    send_tp(3, lambda peer: att_out.at[peer // 2], att_in.at[me])
+    att_in[me] = att_out[chip]
     up_copy.wait()
-    send_tp(4, lambda peer: piece(up_v, peer), up_in.at[me])
-    up_in[me] = up_v[:, my_cols]
+    send_tp(4, lambda peer: piece(up_v, peer), half_of(up_in))
+    up_in[core, me] = up_v[:, my_cols]
     val_copy.wait()
-    ow_copy.wait()
+    pltpu.make_async_copy(
+        ow_pair.at[:, head_rows], ow_pair.at[:, head_rows], local_sems.at[11]
+    ).wait()
+    arrived(16, val_pair)
+    pltpu.make_async_copy(
+        ow_pair.at[:, head_rows], ow_pair.at[:, head_rows], recv_sems.at[17]
+    ).wait()
 
     arrived(3, att_in)
     for t in range(n_tp):
-        lat_f[own * t : own * (t + 1), :] = att_in[t].astype(F32)
-    head_values = dot(lat_f[...].astype(BF16), val_v[...]).astype(BF16)
-
-    for d in order + [0]:
-        peer = lax.rem(me + d, n_tp)
-        share = dot(
-            head_values, ow_v[:, pl.ds(pl.multiple_of(peer * cols, cols), cols)]
-        ).astype(BF16)
+        msg_f[own * t : own * (t + 1), : 2 * latent] = att_in[t].astype(F32)
+    results = msg_f[:, : 2 * latent].astype(BF16)
+    head_values = jnp.concatenate(
+        [dot(results[:, c * latent : (c + 1) * latent], val_pair[c]) for c in range(2)], axis=1
+    ).astype(BF16)
+
+    for d in chip_order + [0]:
+        peer = lax.rem(chip + d, n_chip)
+        share = dot(head_values, ow_pair[peer]).astype(BF16)
         if d:
             mix_out[peer] = share
-            send(mix_out.at[peer], mix_in.at[me], 5, {"tp": peer})
+            send(mix_out.at[peer], mix_in.at[chip], 5, {"tp": 2 * peer + core})
         else:
-            mix_in[me] = share
-
+            mix_in[chip] = share
+
+    arrived(2, gate_in.at[core])
+    send(gate_in.at[core], gate_in.at[core], 13, {"tp": sibling})
     tok_cols = tok_f[:, my_cols]
     my_mix_gain = gain_row(mixg_v, my_first, cols)
     my_expert_gain = gain_row(expg_v, my_first, cols)
 
     arrived(5, mix_in)
     mixed = mix_in[0].astype(F32)
-    for t in range(1, n_tp):
+    for t in range(1, n_chip):
         mixed = mixed + mix_in[t].astype(F32)
     mixed = mixed.astype(BF16).astype(F32)
     scaled = mixed * my_mix_gain
@@ -418,6 +495,8 @@
     )
     sum_in[me] = sums
     send_tp(6, lambda peer: sum_in.at[me], sum_in.at[me])
+    arrived(4, up_in.at[core])
+    send(up_in.at[core], up_in.at[core], 14, {"tp": sibling})
     arrived(6, sum_in)
     sums = sum_in[0]
     for t in range(1, n_tp):
@@ -434,63 +513,121 @@
     route_f[...] = dot(dispatch, expert_in)
     for e in range(n_ep):
         dis_out[e] = route_f[slots * e : slots * (e + 1), :].astype(BF16)
-    send_ep(7, lambda peer: dis_out.at[peer], dis_in.at[group])
-    dis_in[group] = dis_out[group]
+    place = 2 * (group // 2) + core
+
+    def send_tokens(d, _):
+        peer = lax.rem(group + d, n_ep)
+        send(dis_out.at[peer], dis_in.at[place], 7, {"ep": peer, "tp": 2 * chip + side})
+        return 0
+
+    lax.fori_loop(1, n_ep, send_tokens, 0)
+
+    @pl.when(at_home)
+    def _():
+        dis_in[place] = dis_out[group]
+
+    @pl.when(jnp.logical_not(at_home))
+    def _():
+        send(dis_out.at[group], dis_in.at[place], 7, {"tp": sibling})
+
     down_copy.wait()
-    send_tp(8, lambda peer: piece(down_v, peer), down_in.at[me])
-    down_in[me] = down_v[:, my_cols]
-
-    arrived(2, gate_in)
-    arrived(4, up_in)
-    arrived(7, dis_in)
-    for g in range(n_ep):
-        route_f[slots * g : slots * (g + 1), :] = dis_in[g].astype(F32)
-    received = route_f[...].astype(BF16)
+    send_tp(8, lambda peer: piece(down_v, peer), half_of(down_in))
+    down_in[core, me] = down_v[:, my_cols]
+
+    arrived_all(13, gate_in.at[core])
+    arrived_all(14, up_in.at[core])
+    at_home_or_not(7, dis_in, recv_sems)
+    side_rows = half_ep * slots
+    for g in range(half_ep):
+        for c in range(2):
+            at = c * side_rows + slots * g
+            route_f[at : at + slots, :] = dis_in[2 * g + c].astype(F32)
+    received = [
+        route_f[c * side_rows : (c + 1) * side_rows, :].astype(BF16) for c in range(2)
+    ]
     ff = n_tp * ff_dev
-    out_rows = all_slots // n_tp
+    out_rows = side_rows // n_chip
     for n, source in enumerate((gate_in, up_in)):
-        part = dot_t(received, source[...].reshape(ff, cols))
-        part_out[:, :, n * ff : (n + 1) * ff] = part.reshape(n_tp, out_rows, ff).astype(BF16)
-
-    send_tp(9, lambda peer: part_out.at[peer], part_in.at[me])
-    part_in[me] = part_out[me]
+        part = dot_t(received[0], source[0].reshape(ff, cols)) + dot_t(
+            received[1], source[1].reshape(ff, cols)
+        )
+        part_out[:, :, n * ff : (n + 1) * ff] = part.reshape(n_chip, out_rows, ff).astype(BF16)
+
+    send_chips(9, lambda peer: part_out.at[peer], part_in.at[chip])
+    part_in[chip] = part_out[chip]
     arrived(9, part_in)
     both = part_in[0].astype(F32)
-    for t in range(1, n_tp):
+    for t in range(1, n_chip):
         both = both + part_in[t].astype(F32)
     gate, upward = both[:, :ff], both[:, ff:]
-    hid_in[me] = (gate / (1.0 + jnp.exp(-gate)) * upward).astype(BF16)
-
-    send_tp(10, lambda peer: hid_in.at[me], hid_in.at[me])
-    arrived(8, down_in)
+    hid_in[chip] = (gate / (1.0 + jnp.exp(-gate)) * upward).astype(BF16)
+
+    send_chips(10, lambda peer: hid_in.at[chip], hid_in.at[chip])
+    arrived(8, down_in.at[core])
+    send(down_in.at[core], down_in.at[core], 15, {"tp": sibling})
+    arrived_all(15, down_in.at[core])
     arrived(10, hid_in)
-    hidden = hid_in[...].astype(F32).reshape(all_slots, ff).astype(BF16)
-    route_f[...] = dot(hidden, down_in[...].reshape(ff, cols))
-    for g in range(n_ep):
-        ret_out[g] = route_f[slots * g : slots * (g + 1), :].astype(BF16)
-
-    send_ep(11, lambda peer: ret_out.at[peer], ret_in.at[group])
-    ret_in[group] = ret_out[group]
-    arrived(11, ret_in)
+    hidden = hid_in[...].astype(F32).reshape(side_rows, ff).astype(BF16)
+    for c in range(2):
+        at = c * side_rows
+        route_f[at : at + side_rows, :] = dot(hidden, down_in[c].reshape(ff, cols))
+        for g in range(half_ep):
+            at = c * side_rows + slots * g
+            ret_out[2 * g + c] = route_f[at : at + slots, :].astype(BF16)
+
+    def send_back(d, _):
+        source = 2 * lax.rem(group // 2 + d, half_ep) + core
+        for c in range(2):
+            send(
+                ret_out.at[2 * (source // 2) + c],
+                ret_in.at[group],
+                11,
+                {"ep": source, "tp": 2 * chip + c},
+            )
+        return 0
+
+    lax.fori_loop(1, half_ep, send_back, 0)
+
+    @pl.when(at_home)
+    def _():
+        ret_in[group] = ret_out[place]
+        send(ret_out.at[place + 1 - 2 * core], ret_in.at[group], 11, {"tp": sibling})
+
+    @pl.when(jnp.logical_not(at_home))
+    def _():
+        for c in range(2):
+            send(
+                ret_out.at[2 * (group // 2) + c],
+                ret_in.at[group],
+                11,
+                {"ep": 2 * (group // 2) + core, "tp": 2 * chip + c},
+            )
+
+    at_home_or_not(11, ret_in, recv_sems)
     for e in range(n_ep):
         route_f[slots * e : slots * (e + 1), :] = ret_in[e].astype(F32)
     out[...] = (resid + dot(combine, route_f[...], HIGHEST)).astype(BF16)
 
+    sent(0, tok_in)
     for stage, buffer in (
-        (0, tok_in),
         (1, qry_in),
-        (2, gate_in),
+        (2, gate_in.at[core]),
         (3, att_in),
-        (4, up_in),
+        (4, up_in.at[core]),
         (5, mix_in),
         (6, sum_in),
-        (7, dis_in),
-        (8, down_in),
+        (8, down_in.at[core]),
         (9, part_in),
         (10, hid_in),
-        (11, ret_in),
+        (16, val_pair),
     ):
         sent(stage, buffer)
+    sent_all(13, gate_in.at[core])
+    sent_all(14, up_in.at[core])
+    sent_all(15, down_in.at[core])
+    sent_all(17, ow_pair.at[:, head_rows])
+    at_home_or_not(7, dis_in, send_sems)
+    at_home_or_not(11, ret_in, send_sems)
 
 
 def per_device(
@@ -525,6 +662,7 @@
     ff = ff_dev * n_tp
     slots = 2 * rows * expert_ids.shape[1] // n_ep
     all_slots = n_ep * slots
+    n_chip = n_tp // 2
     out_rows = all_slots // n_tp
 
     operands = (
@@ -576,8 +714,8 @@
             vmem(latent_weight.shape, BF16),
             vmem((QK_ROPE, cols), BF16),
             vmem(absorb_weight.shape[1:], BF16),
-            vmem(value_weight.shape[1:], BF16),
-            vmem(output_weight.shape, BF16),
+            vmem((2, *value_weight.shape[1:]), BF16),
+            vmem((n_chip, 2 * output_weight.shape[0], cols), BF16),
             vmem((ff_dev, width), BF16),
             vmem((ff_dev, width), BF16),
             vmem((ff_dev, width), BF16),
@@ -589,24 +727,25 @@
             vmem((n_tp, own, width), BF16),
             vmem((n_tp, own, MESSAGE), BF16),
             vmem((n_tp, own, MESSAGE), BF16),
-            vmem((n_tp, own, latent), BF16),
-            vmem((n_tp, own, latent), BF16),
-            vmem((n_tp, rows, cols), BF16),
-            vmem((n_tp, rows, cols), BF16),
+            vmem((n_chip, own, 2 * latent), BF16),
+            vmem((n_tp, own, 2 * latent), BF16),
+            vmem((n_chip, rows, cols), BF16),
+            vmem((n_chip, rows, cols), BF16),
             vmem((n_tp, 1, 4 * rows), F32),
             vmem((n_ep, slots, cols), BF16),
             vmem((n_ep, slots, cols), BF16),
-            vmem((n_tp, out_rows, 2 * ff), BF16),
-            vmem((n_tp, out_rows, 2 * ff), BF16),
-            vmem((n_tp, out_rows, ff), BF16),
+            vmem((n_chip, out_rows, 2 * ff), BF16),
+            vmem((n_chip, out_rows, 2 * ff), BF16),
+            vmem((n_chip, out_rows, ff), BF16),
             vmem((n_ep, slots, cols), BF16),
             vmem((n_ep, slots, cols), BF16),
-            vmem((n_tp, ff_dev, cols), BF16),
-            vmem((n_tp, ff_dev, cols), BF16),
-            vmem((n_tp, ff_dev, cols), BF16),
+            vmem((2, n_tp, ff_dev, cols), BF16),
+            vmem((2, n_tp, ff_dev, cols), BF16),
+            vmem((2, n_tp, ff_dev, cols), BF16),
             pltpu.SemaphoreType.DMA((20,)),
-            pltpu.SemaphoreType.DMA((12,)),
-            pltpu.SemaphoreType.DMA((12,)),
+            pltpu.SemaphoreType.DMA((18,)),
+            pltpu.SemaphoreType.DMA((18,)),
+            pltpu.SemaphoreType.DMA((n_chip,)),
         ],
         compiler_params=pltpu.CompilerParams(
             collective_id=0, has_side_effects=True, vmem_limit_bytes=67_043_328

time: 80.6 us -> 75.6 us (0.938)
  Pallas kernels: 77.3 us -> 72.3 us
    pallas_call x1, Pallas kernels: 77.3 us -> 72.3 us  [per_device(): pl.pallas_call(functools.partial(kernel, n_tp, n_ep), out_shape=(jax.Shap...]
where the time goes in v3:
time: 75.6 us; the launch traced here: 75.4 us
  Pallas kernels  72.3 us (96%)
  local copies, waits for them, and re-layouts  2.45 us (3%)
    pallas_call x1, Pallas kernels, per_device(): pl.pallas_call(functools.partial(kernel, n_tp, n_ep), out_shape=(jax.Shap...  72.3 us
    unnamed x7, local copies, waits for them, and re-layouts  2.45 us

profile of v3, /device:TPU:1, one launch (start us, length us, event | category | flops | bytes accessed | tf_op | source)
XLA Modules:
  0.0 75.4 jit_solution(12725656057330873651)
XLA Ops:
  0.6 72.3 %shard_map.211 = (bf16[32,256]{1,0:T(8,128)(2,1)}, bf16[2,256]{1,0:T(2,128)(2,1)}, bf16[2,64]{1,0:T(2,128)(2,1)}) custom-call(bf16[2,4096]{1,0:T(2,128)(2,1)} %tokens.1, s32[1,32]{1,0:T(1,128)} %bitcast.15, bf16[2,1024,256]{2,1,0:T(8,128)(2,1)} %latent_cache.1, bf16[2,64,1024]{2,1,0:T(8,128)(2,1)} %bitcast.9, bf16[4096]{0:T(1024)(128)(2,1)} %attn_gain.1, ...), custom_call_target="tpu_custom_call" | custom-call | tf_op jit(solution)/shard_map/pallas_call | solution.py:691
  73.0 0.0 copy-start
  73.0 1.3 %copy.26 = bf16[32,256]{1,0:T(8,128)(2,1)} copy(bf16[32,256]{1,0:T(8,128)(2,1)} %get-tuple-element.6) | data formatting | bytes 32768
  74.3 0.0 copy-done
  74.3 0.0 copy-start.1
  74.3 0.6 copy.27
  74.9 0.0 copy-done.1
  74.9 0.5 copy.28
Async XLA Ops:
  73.0 1.3 %copy-start = (bf16[2,256]{1,0:T(2,128)(2,1)S(1)}, bf16[2,256]{1,0:T(2,128)(2,1)}, u32[]{:S(2)}) copy-start(bf16[2,256]{1,0:T(2,128)(2,1)} %get-tuple-element.7) | copy-start | bytes 3076
  74.3 0.6 copy-start.1

commit v4 on v3

--- a/solution.py
+++ b/solution.py
@@ -86,7 +86,7 @@
     latg_v,
     lat_v,
     rope_v,
-    qw_v,
+    query_v,
     qrw_v,
     lw_v,
     krw_v,
@@ -158,21 +158,15 @@
     for d in range(1, n_tp):
         greet({"tp": lax.rem(me + d, n_tp)})
 
-    def greet_ep(d, _):
+    for d in range(1, n_ep):
         greet({"ep": lax.rem(group + d, n_ep), "tp": 2 * chip + side})
-        return 0
-
-    lax.fori_loop(1, n_ep, greet_ep, 0)
 
     @pl.when(jnp.logical_not(at_home))
     def _():
         greet({"tp": sibling})
 
-    def greet_back(d, _):
+    for d in range(half_ep):
         greet({"ep": 2 * d + core, "tp": 2 * chip + 1 - side})
-        return 0
-
-    lax.fori_loop(0, half_ep, greet_back, 0)
 
     small = [
         load(13, lengths, len_v),
@@ -183,7 +177,7 @@
         load(18, expert_gain, expg_v),
         load(19, latent_gain, latg_v),
     ]
-    qw_copy = load(1, query_weight, qw_v)
+    qw_copy = load(1, query_weight, query_v.at[:, pl.ds(0, QK_NOPE)])
     qrw_copy = load(2, query_rot_weight, qrw_v)
     lw_copy = load(3, latent_weight, lw_v)
     krw_copy = load(4, key_rot_weight, krw_v)
@@ -318,6 +312,10 @@
     own_sine = dot(own_rows, sine, HIGHEST)[:own]
     own_lengths = jnp.sum(own_rows * lengths_row, axis=1, keepdims=True).astype(jnp.int32)
 
+    qrw_copy.wait()
+    for c in range(0, width, 512):
+        query_v[c : c + 512, QK_NOPE : QK_NOPE + QK_ROPE] = qrw_v[:, c : c + 512].T
+    qw_copy.wait()
     for d in reversed(chip_order):
         peer = lax.rem(chip + d, n_chip)
         slot = tok_in.at[2 * peer + core]
@@ -336,12 +334,11 @@
         x = tok_f[:, c : c + chunk]
         normed_b[:, c : c + chunk] = (x * factor * gain_row(attn_v, c, chunk)).astype(BF16)
 
-    qw_copy.wait()
-    q_nope = dot(normed_b[...], qw_v[...]).astype(BF16)
+    query = dot(normed_b[...], query_v[...])
+    q_nope = query[:, :QK_NOPE].astype(BF16)
+    q_rot = query[:, QK_NOPE : QK_NOPE + QK_ROPE]
     abs_copy.wait()
     msg_f[:, LAT_AT : LAT_AT + latent] = dot(q_nope, abs_v[...])
-    qrw_copy.wait()
-    q_rot = dot_t(normed_b[...], qrw_v[...])
     msg_f[:, ROT_AT : ROT_AT + QK_ROPE] = q_rot * cosine + swap_halves(q_rot) * sine
     slice_rows = normed_b[:, my_cols]
     lw_copy.wait()
@@ -515,12 +512,9 @@
         dis_out[e] = route_f[slots * e : slots * (e + 1), :].astype(BF16)
     place = 2 * (group // 2) + core
 
-    def send_tokens(d, _):
+    for d in range(1, n_ep):
         peer = lax.rem(group + d, n_ep)
         send(dis_out.at[peer], dis_in.at[place], 7, {"ep": peer, "tp": 2 * chip + side})
-        return 0
-
-    lax.fori_loop(1, n_ep, send_tokens, 0)
 
     @pl.when(at_home)
     def _():
@@ -575,18 +569,15 @@
             at = c * side_rows + slots * g
             ret_out[2 * g + c] = route_f[at : at + slots, :].astype(BF16)
 
-    def send_back(d, _):
-        source = 2 * lax.rem(group // 2 + d, half_ep) + core
+    for d in range(1, half_ep):
+        pair = lax.rem(group // 2 + d, half_ep)
         for c in range(2):
             send(
-                ret_out.at[2 * (source // 2) + c],
+                ret_out.at[2 * pair + c],
                 ret_in.at[group],
                 11,
-                {"ep": source, "tp": 2 * chip + c},
+                {"ep": 2 * pair + core, "tp": 2 * chip + c},
             )
-        return 0
-
-    lax.fori_loop(1, half_ep, send_back, 0)
 
     @pl.when(at_home)
     def _():
@@ -628,6 +619,21 @@
     sent_all(17, ow_pair.at[:, head_rows])
     at_home_or_not(7, dis_in, send_sems)
     at_home_or_not(11, ret_in, send_sems)
+
+
+def hand_over(*refs):
+    sources, targets, held, sems = refs[:3], refs[3:6], refs[6:9], refs[9]
+    inward = [pltpu.make_async_copy(a, b, sems.at[i]) for i, (a, b) in enumerate(zip(sources, held))]
+    outward = [
+        pltpu.make_async_copy(a, b, sems.at[3 + i]) for i, (a, b) in enumerate(zip(held, targets))
+    ]
+    for copy in inward:
+        copy.start()
+    for before, copy in zip(inward, outward):
+        before.wait()
+        copy.start()
+    for copy in outward:
+        copy.wait()
 
 
 def per_device(
@@ -688,13 +694,14 @@
         route_weights.T,
     )
     vmem = pltpu.VMEM
-    return pl.pallas_call(
+    shapes = (
+        jax.ShapeDtypeStruct((rows, cols), BF16),
+        jax.ShapeDtypeStruct((own, latent), BF16),
+        jax.ShapeDtypeStruct((own, QK_ROPE), BF16),
+    )
+    results = pl.pallas_call(
         functools.partial(kernel, n_tp, n_ep),
-        out_shape=(
-            jax.ShapeDtypeStruct((rows, cols), BF16),
-            jax.ShapeDtypeStruct((own, latent), BF16),
-            jax.ShapeDtypeStruct((own, QK_ROPE), BF16),
-        ),
+        out_shape=shapes,
         in_specs=[
             pl.BlockSpec(memory_space=pl.ANY) for _ in operands
         ],
@@ -709,7 +716,7 @@
             vmem((latent,), BF16),
             vmem(latent_cache.shape, BF16),
             vmem((own, QK_ROPE, context), BF16),
-            vmem(query_weight.shape, BF16),
+            vmem((width, QK_NOPE + QK_ROPE), BF16),
             vmem((QK_ROPE, width), BF16),
             vmem(latent_weight.shape, BF16),
             vmem((QK_ROPE, cols), BF16),
@@ -751,6 +758,14 @@
             collective_id=0, has_side_effects=True, vmem_limit_bytes=67_043_328
         ),
     )(*operands)
+    return pl.pallas_call(
+        hand_over,
+        out_shape=shapes,
+        in_specs=[pl.BlockSpec(memory_space=pl.ANY)] * 3,
+        out_specs=[pl.BlockSpec(memory_space=pl.ANY)] * 3,
+        scratch_shapes=[vmem(x.shape, BF16) for x in shapes] + [pltpu.SemaphoreType.DMA((6,))],
+        compiler_params=pltpu.CompilerParams(vmem_limit_bytes=67_043_328),
+    )(*results)
 
 
 def solution(mesh):

time: 75.6 us -> 74.4 us (0.984)
  local copies, waits for them, and re-layouts: 2.45 us -> 0 us
  Pallas kernels: 72.3 us -> 73.5 us
    unnamed x7 -> x0, local copies, waits for them, and re-layouts: 2.45 us -> none
    pallas_call x1 -> x2, Pallas kernels: 72.3 us -> 73.5 us  [the longest x1 72.1 us: per_device(): pl.pallas_call(functools.partial(kernel, n_tp, n_ep), out_shape=shapes, i...]
where the time goes in v4:
time: 74.4 us; the launch traced here: 74.2 us
  Pallas kernels  73.5 us (99%)
    pallas_call x1, Pallas kernels, per_device(): pl.pallas_call(functools.partial(kernel, n_tp, n_ep), out_shape=shapes, i...  72.1 us

profile of v4, /device:TPU:1, one launch (start us, length us, event | category | flops | bytes accessed | tf_op | source)
XLA Modules:
  0.0 74.2 jit_solution(11171696587060543147)
XLA Ops:
  0.6 72.1 %shard_map.211 = (bf16[32,256]{1,0:T(8,128)(2,1)}, bf16[2,256]{1,0:T(2,128)(2,1)}, bf16[2,64]{1,0:T(2,128)(2,1)}) custom-call(bf16[2,4096]{1,0:T(2,128)(2,1)} %tokens.1, s32[1,32]{1,0:T(1,128)} %bitcast.15, bf16[2,1024,256]{2,1,0:T(8,128)(2,1)} %latent_cache.1, bf16[2,64,1024]{2,1,0:T(8,128)(2,1)} %bitcast.9, bf16[4096]{0:T(1024)(128)(2,1)} %attn_gain.1, ...), custom_call_target="tpu_custom_call" | custom-call | tf_op jit(solution)/shard_map/pallas_call | solution.py:702
  72.8 1.4 %shard_map.212 = (bf16[32,256]{1,0:T(8,128)(2,1)}, bf16[2,256]{1,0:T(2,128)(2,1)}, bf16[2,64]{1,0:T(2,128)(2,1)}) custom-call(bf16[32,256]{1,0:T(8,128)(2,1)} %get-tuple-element.6.refs_0_, bf16[2,256]{1,0:T(2,128)(2,1)} %get-tuple-element.7.refs_1_, bf16[2,64]{1,0:T(2,128)(2,1)} %get-tuple-element.8.refs_2_), custom_call_target="tpu_custom_call" | custom-call | tf_op jit(solution)/shard_map/pallas_call | solution.py:761

commit v5 on v4

--- a/solution.py
+++ b/solution.py
@@ -334,7 +334,8 @@
         x = tok_f[:, c : c + chunk]
         normed_b[:, c : c + chunk] = (x * factor * gain_row(attn_v, c, chunk)).astype(BF16)
 
-    query = dot(normed_b[...], query_v[...])
+    mid = width // 2
+    query = dot(normed_b[:, :mid], query_v[:mid]) + dot(normed_b[:, mid:], query_v[mid:])
     q_nope = query[:, :QK_NOPE].astype(BF16)
     q_rot = query[:, QK_NOPE : QK_NOPE + QK_ROPE]
     abs_copy.wait()
@@ -450,14 +451,13 @@
         [dot(results[:, c * latent : (c + 1) * latent], val_pair[c]) for c in range(2)], axis=1
     ).astype(BF16)
 
-    for d in chip_order + [0]:
-        peer = lax.rem(chip + d, n_chip)
-        share = dot(head_values, ow_pair[peer]).astype(BF16)
-        if d:
-            mix_out[peer] = share
+    for batch in (chip_order[:3], chip_order[3:]):
+        peers = [lax.rem(chip + d, n_chip) for d in batch]
+        for peer in peers:
+            mix_out[peer] = dot(head_values, ow_pair[peer]).astype(BF16)
+        for peer in peers:
             send(mix_out.at[peer], mix_in.at[chip], 5, {"tp": 2 * peer + core})
-        else:
-            mix_in[chip] = share
+    mix_in[chip] = dot(head_values, ow_pair[chip]).astype(BF16)
 
     arrived(2, gate_in.at[core])
     send(gate_in.at[core], gate_in.at[core], 13, {"tp": sibling})
@@ -622,17 +622,13 @@
 
 
 def hand_over(*refs):
-    sources, targets, held, sems = refs[:3], refs[3:6], refs[6:9], refs[9]
-    inward = [pltpu.make_async_copy(a, b, sems.at[i]) for i, (a, b) in enumerate(zip(sources, held))]
-    outward = [
-        pltpu.make_async_copy(a, b, sems.at[3 + i]) for i, (a, b) in enumerate(zip(held, targets))
+    sources, targets, sems = refs[:3], refs[3:6], refs[6]
+    copies = [
+        pltpu.make_async_copy(a, b, sems.at[i]) for i, (a, b) in enumerate(zip(sources, targets))
     ]
-    for copy in inward:
+    for copy in copies:
         copy.start()
-    for before, copy in zip(inward, outward):
-        before.wait()
-        copy.start()
-    for copy in outward:
+    for copy in copies:
         copy.wait()
 
 
@@ -703,7 +699,7 @@
         functools.partial(kernel, n_tp, n_ep),
         out_shape=shapes,
         in_specs=[
-            pl.BlockSpec(memory_space=pl.ANY) for _ in operands
+            pl.BlockSpec(memory_space=pltpu.HBM) for _ in operands
         ],
         out_specs=[pl.BlockSpec(memory_space=vmem)] * 3,
         scratch_shapes=[
@@ -755,16 +751,16 @@
             pltpu.SemaphoreType.DMA((n_chip,)),
         ],
         compiler_params=pltpu.CompilerParams(
-            collective_id=0, has_side_effects=True, vmem_limit_bytes=67_043_328
+            collective_id=0, has_side_effects=True, vmem_limit_bytes=40 * 1024 * 1024
         ),
-    )(*operands)
+    )(*[pltpu.with_memory_space_constraint(x, pltpu.HBM) for x in operands])
     return pl.pallas_call(
         hand_over,
         out_shape=shapes,
-        in_specs=[pl.BlockSpec(memory_space=pl.ANY)] * 3,
-        out_specs=[pl.BlockSpec(memory_space=pl.ANY)] * 3,
-        scratch_shapes=[vmem(x.shape, BF16) for x in shapes] + [pltpu.SemaphoreType.DMA((6,))],
-        compiler_params=pltpu.CompilerParams(vmem_limit_bytes=67_043_328),
+        in_specs=[pl.BlockSpec(memory_space=vmem)] * 3,
+        out_specs=[pl.BlockSpec(memory_space=pltpu.HBM)] * 3,
+        scratch_shapes=[pltpu.SemaphoreType.DMA((3,))],
+        compiler_params=pltpu.CompilerParams(vmem_limit_bytes=16 * 1024 * 1024),
     )(*results)
 
 

time: 74.4 us -> 73 us (0.981)
  Pallas kernels: 73.5 us -> 72.3 us
where the time goes in v5:
time: 73 us; the launch traced here: 72.9 us
  Pallas kernels  72.3 us (99%)
    pallas_call x1, Pallas kernels, per_device(): pl.pallas_call(functools.partial(kernel, n_tp, n_ep), out_shape=shapes, i...  71.6 us

profile of v5, /device:TPU:1, one launch (start us, length us, event | category | flops | bytes accessed | tf_op | source)
XLA Modules:
  0.0 72.9 jit_solution(17010782562256686140)
XLA Ops:
  0.6 71.6 %shard_map.211 = (bf16[32,256]{1,0:T(8,128)(2,1)S(1)}, bf16[2,256]{1,0:T(2,128)(2,1)S(1)}, bf16[2,64]{1,0:T(2,128)(2,1)S(1)}) custom-call(bf16[2,4096]{1,0:T(2,128)(2,1)} %tokens.1, s32[1,32]{1,0:T(1,128)} %bitcast.15, bf16[2,1024,256]{2,1,0:T(8,128)(2,1)} %latent_cache.1, bf16[2,64,1024]{2,1,0:T(8,128)(2,1)} %bitcast.9, bf16[4096]{0:T(1024)(128)(2,1)} %attn_gain.1, ...), custom_call_target="tpu_custom_call" | custom-call | tf_op jit(solution)/shard_map/pallas_call | solution.py:698
  72.3 0.6 shard_map.212

commit v6 on v5

--- a/solution.py
+++ b/solution.py
@@ -101,6 +101,7 @@
     msg_f,
     lat_f,
     route_f,
+    factor_f,
     tok_in,
     qry_out,
     qry_in,
@@ -113,6 +114,12 @@
     dis_in,
     part_out,
     part_in,
+    tok_dis_out,
+    tok_dis_in,
+    tok_part_out,
+    tok_part_in,
+    factor_out,
+    factor_in,
     hid_in,
     ret_out,
     ret_in,
@@ -370,6 +377,29 @@
     send_tp(2, lambda peer: piece(gate_v, peer), half_of(gate_in))
     gate_in[core, me] = gate_v[:, my_cols]
 
+    tok_cols = tok_f[:, my_cols]
+    my_mix_gain = gain_row(mixg_v, my_first, cols)
+    my_expert_gain = gain_row(expg_v, my_first, cols)
+    place = 2 * (group // 2) + core
+
+    def to_experts(stage, value, out_ref, in_ref):
+        route_f[...] = dot(dispatch, value.astype(BF16))
+        for e in range(n_ep):
+            out_ref[e] = route_f[slots * e : slots * (e + 1), :].astype(BF16)
+        for d in range(1, n_ep):
+            peer = lax.rem(group + d, n_ep)
+            send(out_ref.at[peer], in_ref.at[place], stage, {"ep": peer, "tp": 2 * chip + side})
+
+        @pl.when(at_home)
+        def _():
+            in_ref[place] = out_ref[group]
+
+        @pl.when(jnp.logical_not(at_home))
+        def _():
+            send(out_ref.at[group], in_ref.at[place], stage, {"tp": sibling})
+
+    to_experts(18, tok_cols * my_expert_gain, tok_dis_out, tok_dis_in)
+
     lat_copy.wait()
     rope_copy.wait()
 
@@ -461,9 +491,38 @@
 
     arrived(2, gate_in.at[core])
     send(gate_in.at[core], gate_in.at[core], 13, {"tp": sibling})
-    tok_cols = tok_f[:, my_cols]
-    my_mix_gain = gain_row(mixg_v, my_first, cols)
-    my_expert_gain = gain_row(expg_v, my_first, cols)
+    arrived(4, up_in.at[core])
+    send(up_in.at[core], up_in.at[core], 14, {"tp": sibling})
+    side_rows = half_ep * slots
+    ff = n_tp * ff_dev
+    out_rows = side_rows // n_chip
+
+    def partial_sums(in_ref, out_ref):
+        for g in range(half_ep):
+            for c in range(2):
+                at = c * side_rows + slots * g
+                route_f[at : at + slots, :] = in_ref[2 * g + c].astype(F32)
+        received = [
+            route_f[c * side_rows : (c + 1) * side_rows, :].astype(BF16) for c in range(2)
+        ]
+        for n, source in enumerate((gate_in, up_in)):
+            part = dot_t(received[0], source[0].reshape(ff, cols)) + dot_t(
+                received[1], source[1].reshape(ff, cols)
+            )
+            out_ref[:, :, n * ff : (n + 1) * ff] = part.reshape(n_chip, out_rows, ff).astype(BF16)
+
+    def summed_parts(in_ref):
+        both = in_ref[0].astype(F32)
+        for t in range(1, n_chip):
+            both = both + in_ref[t].astype(F32)
+        return both
+
+    at_home_or_not(18, tok_dis_in, recv_sems)
+    arrived_all(13, gate_in.at[core])
+    arrived_all(14, up_in.at[core])
+    partial_sums(tok_dis_in, tok_part_out)
+    send_chips(19, lambda peer: tok_part_out.at[peer], tok_part_in.at[chip])
+    tok_part_in[chip] = tok_part_out[chip]
 
     arrived(5, mix_in)
     mixed = mix_in[0].astype(F32)
@@ -471,6 +530,8 @@
         mixed = mixed + mix_in[t].astype(F32)
     mixed = mixed.astype(BF16).astype(F32)
     scaled = mixed * my_mix_gain
+
+    to_experts(7, scaled * my_expert_gain, dis_out, dis_in)
 
     def as_row(col):
         return jnp.sum(eye * col, axis=0, keepdims=True)
@@ -492,8 +553,10 @@
     )
     sum_in[me] = sums
     send_tp(6, lambda peer: sum_in.at[me], sum_in.at[me])
-    arrived(4, up_in.at[core])
-    send(up_in.at[core], up_in.at[core], 14, {"tp": sibling})
+    down_copy.wait()
+    send_tp(8, lambda peer: piece(down_v, peer), half_of(down_in))
+    down_in[core, me] = down_v[:, my_cols]
+
     arrived(6, sum_in)
     sums = sum_in[0]
     for t in range(1, n_tp):
@@ -505,54 +568,44 @@
     resid = (tok_cols + scaled * mix_factor).astype(BF16).astype(F32)
     resid_square = square_sum + mix_factor * (2.0 * cross + mix_factor * scaled_square)
     resid_factor = lax.rsqrt(jnp.maximum(resid_square, 0.0) / width + norm_floor)
-    expert_in = (resid * resid_factor * my_expert_gain).astype(BF16)
-
-    route_f[...] = dot(dispatch, expert_in)
+
+    lanes = iota((rows, 128), 1)
+    factors = jnp.where(lanes < 64, mix_factor, resid_factor)
+    factor_f[...] = dot(dispatch.astype(F32), factors, HIGHEST)
     for e in range(n_ep):
-        dis_out[e] = route_f[slots * e : slots * (e + 1), :].astype(BF16)
-    place = 2 * (group // 2) + core
-
-    for d in range(1, n_ep):
-        peer = lax.rem(group + d, n_ep)
-        send(dis_out.at[peer], dis_in.at[place], 7, {"ep": peer, "tp": 2 * chip + side})
-
-    @pl.when(at_home)
+        factor_out[e] = factor_f[slots * e : slots * (e + 1), :]
+    per_device_groups = out_rows // slots
+    speaks = me == 2 * (group // (2 * per_device_groups)) + side
+    factor_place = lax.rem(group // 2, per_device_groups)
+
+    @pl.when(speaks)
     def _():
-        dis_in[place] = dis_out[group]
-
-    @pl.when(jnp.logical_not(at_home))
-    def _():
-        send(dis_out.at[group], dis_in.at[place], 7, {"tp": sibling})
-
-    down_copy.wait()
-    send_tp(8, lambda peer: piece(down_v, peer), half_of(down_in))
-    down_in[core, me] = down_v[:, my_cols]
-
-    arrived_all(13, gate_in.at[core])
-    arrived_all(14, up_in.at[core])
+        for d in range(1, n_ep):
+            peer = lax.rem(group + d, n_ep)
+            send(factor_out.at[peer], factor_in.at[factor_place], 20, {"ep": peer})
+        factor_in[factor_place] = factor_out[group]
+
     at_home_or_not(7, dis_in, recv_sems)
-    side_rows = half_ep * slots
-    for g in range(half_ep):
-        for c in range(2):
-            at = c * side_rows + slots * g
-            route_f[at : at + slots, :] = dis_in[2 * g + c].astype(F32)
-    received = [
-        route_f[c * side_rows : (c + 1) * side_rows, :].astype(BF16) for c in range(2)
-    ]
-    ff = n_tp * ff_dev
-    out_rows = side_rows // n_chip
-    for n, source in enumerate((gate_in, up_in)):
-        part = dot_t(received[0], source[0].reshape(ff, cols)) + dot_t(
-            received[1], source[1].reshape(ff, cols)
-        )
-        part_out[:, :, n * ff : (n + 1) * ff] = part.reshape(n_chip, out_rows, ff).astype(BF16)
+    partial_sums(dis_in, part_out)
 
     send_chips(9, lambda peer: part_out.at[peer], part_in.at[chip])
     part_in[chip] = part_out[chip]
     arrived(9, part_in)
-    both = part_in[0].astype(F32)
-    for t in range(1, n_chip):
-        both = both + part_in[t].astype(F32)
+    arrived(19, tok_part_in)
+
+    @pl.when(speaks)
+    def _():
+        wait_for(recv_sems.at[20], factor_in, per_device_groups - 1)
+
+    @pl.when(jnp.logical_not(speaks))
+    def _():
+        wait_for(recv_sems.at[20], factor_in, per_device_groups)
+
+    for g in range(per_device_groups):
+        factor_f[slots * g : slots * (g + 1), :] = factor_in[g]
+    mix_factors = factor_f[:out_rows, 0:1]
+    resid_factors = factor_f[:out_rows, 64:65]
+    both = (summed_parts(tok_part_in) + mix_factors * summed_parts(part_in)) * resid_factors
     gate, upward = both[:, :ff], both[:, ff:]
     hid_in[chip] = (gate / (1.0 + jnp.exp(-gate)) * upward).astype(BF16)
 
@@ -611,6 +664,7 @@
         (9, part_in),
         (10, hid_in),
         (16, val_pair),
+        (19, tok_part_in),
     ):
         sent(stage, buffer)
     sent_all(13, gate_in.at[core])
@@ -618,6 +672,12 @@
     sent_all(15, down_in.at[core])
     sent_all(17, ow_pair.at[:, head_rows])
     at_home_or_not(7, dis_in, send_sems)
+    at_home_or_not(18, tok_dis_in, send_sems)
+
+    @pl.when(speaks)
+    def _():
+        sent(20, factor_out)
+
     at_home_or_not(11, ret_in, send_sems)
 
 
@@ -727,6 +787,7 @@
             vmem((rows, MESSAGE), F32),
             vmem((rows, latent), F32),
             vmem((all_slots, cols), F32),
+            vmem((all_slots, 128), F32),
             vmem((n_tp, own, width), BF16),
             vmem((n_tp, own, MESSAGE), BF16),
             vmem((n_tp, own, MESSAGE), BF16),
@@ -739,6 +800,12 @@
             vmem((n_ep, slots, cols), BF16),
             vmem((n_chip, out_rows, 2 * ff), BF16),
             vmem((n_chip, out_rows, 2 * ff), BF16),
+            vmem((n_ep, slots, cols), BF16),
+            vmem((n_ep, slots, cols), BF16),
+            vmem((n_chip, out_rows, 2 * ff), BF16),
+            vmem((n_chip, out_rows, 2 * ff), BF16),
+            vmem((n_ep, slots, 128), F32),
+            vmem((out_rows // slots, slots, 128), F32),
             vmem((n_chip, out_rows, ff), BF16),
             vmem((n_ep, slots, cols), BF16),
             vmem((n_ep, slots, cols), BF16),
@@ -746,8 +813,8 @@
             vmem((2, n_tp, ff_dev, cols), BF16),
             vmem((2, n_tp, ff_dev, cols), BF16),
             pltpu.SemaphoreType.DMA((20,)),
-            pltpu.SemaphoreType.DMA((18,)),
-            pltpu.SemaphoreType.DMA((18,)),
+            pltpu.SemaphoreType.DMA((21,)),
+            pltpu.SemaphoreType.DMA((21,)),
             pltpu.SemaphoreType.DMA((n_chip,)),
         ],
         compiler_params=pltpu.CompilerParams(

time: 73 us -> 69.5 us (0.952)
  Pallas kernels: 72.3 us -> 68.8 us
    pallas_call x1, Pallas kernels: 71.6 us -> 68.1 us  [per_device(): pl.pallas_call(functools.partial(kernel, n_tp, n_ep), out_shape=shapes, i...]
where the time goes in v6:
time: 69.5 us; the launch traced here: 69.4 us
  Pallas kernels  68.8 us (99%)
    pallas_call x1, Pallas kernels, per_device(): pl.pallas_call(functools.partial(kernel, n_tp, n_ep), out_shape=shapes, i...  68.1 us

profile of v6, /device:TPU:1, one launch (start us, length us, event | category | flops | bytes accessed | tf_op | source)
XLA Modules:
  0.0 69.4 jit_solution(9719622439802689558)
XLA Ops:
  0.6 68.1 %shard_map.211 = (bf16[32,256]{1,0:T(8,128)(2,1)S(1)}, bf16[2,256]{1,0:T(2,128)(2,1)S(1)}, bf16[2,64]{1,0:T(2,128)(2,1)S(1)}) custom-call(bf16[2,4096]{1,0:T(2,128)(2,1)} %tokens.1, s32[1,32]{1,0:T(1,128)} %bitcast.15, bf16[2,1024,256]{2,1,0:T(8,128)(2,1)} %latent_cache.1, bf16[2,64,1024]{2,1,0:T(8,128)(2,1)} %bitcast.9, bf16[4096]{0:T(1024)(128)(2,1)} %attn_gain.1, ...), custom_call_target="tpu_custom_call" | custom-call | tf_op jit(solution)/shard_map/pallas_call | solution.py:758
  68.8 0.6 shard_map.212

commit v7 on v6

--- a/solution.py
+++ b/solution.py
@@ -18,6 +18,9 @@
 norm_floor = 1e-06
 rope_base = 10000.0
 masked_score = -1e30
+
+EP_X = 4
+GATE_NEAR, UP_NEAR, DOWN_NEAR = 5, 4, 4
 
 LAT_AT, KEY_AT, ROT_AT, KEY_ROT_AT, MESSAGE = 0, 256, 512, 640, 768
 
@@ -162,11 +165,21 @@
     def greet(device):
         pl.semaphore_signal(barrier, inc=1, device_id=device, device_id_type=MESH)
 
+    n_z = n_ep // EP_X
+    group_z, group_x = group // EP_X, lax.rem(group, EP_X)
+    ep_order = sorted(
+        [(z, x) for z in range(n_z) for x in range(EP_X) if z or x],
+        key=lambda o: -min(o[0], n_z - o[0]) - min(o[1], EP_X - o[1]),
+    )
+
+    def ep_peer(offset):
+        return EP_X * lax.rem(group_z + offset[0], n_z) + lax.rem(group_x + offset[1], EP_X)
+
+    for offset in ep_order:
+        greet({"ep": ep_peer(offset), "tp": 2 * chip + side})
+
     for d in range(1, n_tp):
         greet({"tp": lax.rem(me + d, n_tp)})
-
-    for d in range(1, n_ep):
-        greet({"ep": lax.rem(group + d, n_ep), "tp": 2 * chip + side})
 
     @pl.when(jnp.logical_not(at_home))
     def _():
@@ -228,7 +241,7 @@
     def send_tp(stage, src_of, dst):
         for d in order:
             peer = lax.rem(me + d, n_tp)
-            send(src_of(peer), dst(peer) if callable(dst) else dst, stage, {"tp": peer})
+            send(src_of(peer), dst, stage, {"tp": peer})
 
     def send_chips(stage, src_of, dst):
         for d in chip_order:
@@ -267,6 +280,25 @@
     for d in chip_order:
         peer = lax.rem(chip + d, n_chip)
         send(tok_in.at[me], tok_in.at[me], 0, {"tp": 2 * peer + core}, tok_sems.at[chip])
+
+    def near_of(limit):
+        return [d for d in order if min(d, n_tp - d) <= limit]
+
+    def far_of(limit):
+        return [d for d in order if min(d, n_tp - d) > limit]
+
+    def send_weights(stage, source, target, offsets):
+        for d in offsets:
+            peer = lax.rem(me + d, n_tp)
+            send(
+                source.at[:, block(peer)],
+                target.at[lax.rem(peer, 2), me],
+                stage,
+                {"tp": peer},
+            )
+
+    gate_copy.wait()
+    send_weights(2, gate_v, gate_in, near_of(GATE_NEAR))
 
     square = (rows, rows)
     eye = (iota(square, 0) == iota(square, 1)).astype(F32)
@@ -321,7 +353,8 @@
 
     qrw_copy.wait()
     for c in range(0, width, 512):
-        query_v[c : c + 512, QK_NOPE : QK_NOPE + QK_ROPE] = qrw_v[:, c : c + 512].T
+        turned = qrw_v[:, c : c + 512].T
+        query_v[c : c + 512, QK_NOPE:] = jnp.concatenate([turned, turned], axis=1)
     qw_copy.wait()
     for d in reversed(chip_order):
         peer = lax.rem(chip + d, n_chip)
@@ -366,15 +399,9 @@
             17,
             {"tp": sibling},
         )
-    gate_copy.wait()
-
-    def piece(ref, peer):
-        return ref.at[:, pl.ds(pl.multiple_of(peer * cols, cols), cols)]
-
-    def half_of(ref):
-        return lambda peer: ref.at[lax.rem(peer, 2), me]
-
-    send_tp(2, lambda peer: piece(gate_v, peer), half_of(gate_in))
+    send_weights(2, gate_v, gate_in, far_of(GATE_NEAR))
+    up_copy.wait()
+    send_weights(4, up_v, up_in, near_of(UP_NEAR))
     gate_in[core, me] = gate_v[:, my_cols]
 
     tok_cols = tok_f[:, my_cols]
@@ -386,8 +413,8 @@
         route_f[...] = dot(dispatch, value.astype(BF16))
         for e in range(n_ep):
             out_ref[e] = route_f[slots * e : slots * (e + 1), :].astype(BF16)
-        for d in range(1, n_ep):
-            peer = lax.rem(group + d, n_ep)
+        for offset in ep_order:
+            peer = ep_peer(offset)
             send(out_ref.at[peer], in_ref.at[place], stage, {"ep": peer, "tp": 2 * chip + side})
 
         @pl.when(at_home)
@@ -461,8 +488,9 @@
 
     send_tp(3, lambda peer: att_out.at[peer // 2], att_in.at[me])
     att_in[me] = att_out[chip]
-    up_copy.wait()
-    send_tp(4, lambda peer: piece(up_v, peer), half_of(up_in))
+    send_weights(4, up_v, up_in, far_of(UP_NEAR))
+    down_copy.wait()
+    send_weights(8, down_v, down_in, near_of(DOWN_NEAR))
     up_in[core, me] = up_v[:, my_cols]
     val_copy.wait()
     pltpu.make_async_copy(
@@ -553,8 +581,7 @@
     )
     sum_in[me] = sums
     send_tp(6, lambda peer: sum_in.at[me], sum_in.at[me])
-    down_copy.wait()
-    send_tp(8, lambda peer: piece(down_v, peer), half_of(down_in))
+    send_weights(8, down_v, down_in, far_of(DOWN_NEAR))
     down_in[core, me] = down_v[:, my_cols]
 
     arrived(6, sum_in)
@@ -580,8 +607,8 @@
 
     @pl.when(speaks)
     def _():
-        for d in range(1, n_ep):
-            peer = lax.rem(group + d, n_ep)
+        for offset in ep_order:
+            peer = ep_peer(offset)
             send(factor_out.at[peer], factor_in.at[factor_place], 20, {"ep": peer})
         factor_in[factor_place] = factor_out[group]
 
@@ -590,6 +617,8 @@
 
     send_chips(9, lambda peer: part_out.at[peer], part_in.at[chip])
     part_in[chip] = part_out[chip]
+    arrived(8, down_in.at[core])
+    send(down_in.at[core], down_in.at[core], 15, {"tp": sibling})
     arrived(9, part_in)
     arrived(19, tok_part_in)
 
@@ -610,8 +639,6 @@
     hid_in[chip] = (gate / (1.0 + jnp.exp(-gate)) * upward).astype(BF16)
 
     send_chips(10, lambda peer: hid_in.at[chip], hid_in.at[chip])
-    arrived(8, down_in.at[core])
-    send(down_in.at[core], down_in.at[core], 15, {"tp": sibling})
     arrived_all(15, down_in.at[core])
     arrived(10, hid_in)
     hidden = hid_in[...].astype(F32).reshape(side_rows, ff).astype(BF16)
@@ -622,8 +649,18 @@
             at = c * side_rows + slots * g
             ret_out[2 * g + c] = route_f[at : at + slots, :].astype(BF16)
 
-    for d in range(1, half_ep):
-        pair = lax.rem(group // 2 + d, half_ep)
+    for z in sorted(range(1, n_z), key=lambda z: -min(z, n_z - z)):
+        for x in range(EP_X // 2):
+            pair = EP_X // 2 * lax.rem(group_z + z, n_z) + x
+            for c in range(2):
+                send(
+                    ret_out.at[2 * pair + c],
+                    ret_in.at[group],
+                    11,
+                    {"ep": 2 * pair + core, "tp": 2 * chip + c},
+                )
+    for x in range(1, EP_X // 2):
+        pair = EP_X // 2 * group_z + lax.rem(group_x // 2 + x, EP_X // 2)
         for c in range(2):
             send(
                 ret_out.at[2 * pair + c],
@@ -772,7 +809,7 @@
             vmem((latent,), BF16),
             vmem(latent_cache.shape, BF16),
             vmem((own, QK_ROPE, context), BF16),
-            vmem((width, QK_NOPE + QK_ROPE), BF16),
+            vmem((width, 2 * QK_NOPE), BF16),
             vmem((QK_ROPE, width), BF16),
             vmem(latent_weight.shape, BF16),
             vmem((QK_ROPE, cols), BF16),

time: 69.5 us -> 67.7 us (0.974)
  Pallas kernels: 68.8 us -> 67 us
    pallas_call x1, Pallas kernels: 68.1 us -> 66.3 us  [per_device(): pl.pallas_call(functools.partial(kernel, n_tp, n_ep), out_shape=shapes, i...]
where the time goes in v7:
time: 67.7 us; the launch traced here: 67.6 us
  Pallas kernels  67 us (99%)
    pallas_call x1, Pallas kernels, per_device(): pl.pallas_call(functools.partial(kernel, n_tp, n_ep), out_shape=shapes, i...  66.3 us

profile of v7, /device:TPU:1, one launch (start us, length us, event | category | flops | bytes accessed | tf_op | source)
XLA Modules:
  0.0 67.6 jit_solution(4554349977000355893)
XLA Ops:
  0.6 66.3 %shard_map.211 = (bf16[32,256]{1,0:T(8,128)(2,1)S(1)}, bf16[2,256]{1,0:T(2,128)(2,1)S(1)}, bf16[2,64]{1,0:T(2,128)(2,1)S(1)}) custom-call(bf16[2,4096]{1,0:T(2,128)(2,1)} %tokens.1, s32[1,32]{1,0:T(1,128)} %bitcast.15, bf16[2,1024,256]{2,1,0:T(8,128)(2,1)} %latent_cache.1, bf16[2,64,1024]{2,1,0:T(8,128)(2,1)} %bitcast.9, bf16[4096]{0:T(1024)(128)(2,1)} %attn_gain.1, ...), custom_call_target="tpu_custom_call" | custom-call | tf_op jit(solution)/shard_map/pallas_call | solution.py:795
  67.0 0.6 shard_map.212

commit v8 on v7

--- a/solution.py
+++ b/solution.py
@@ -22,7 +22,7 @@
 EP_X = 4
 GATE_NEAR, UP_NEAR, DOWN_NEAR = 5, 4, 4
 
-LAT_AT, KEY_AT, ROT_AT, KEY_ROT_AT, MESSAGE = 0, 256, 512, 640, 768
+LAT_AT, KEY_AT, ROT_AT, KEY_ROT_AT, MESSAGE = 0, 256, 512, 576, 640
 
 
 def dot(a, b, precision=None):

time: 67.7 us -> 68.5 us (1.012)
  Pallas kernels: 67 us -> 67.7 us
    pallas_call x1, Pallas kernels: 66.3 us -> 67.1 us  [per_device(): pl.pallas_call(functools.partial(kernel, n_tp, n_ep), out_shape=shapes, i...]
where the time goes in v8:
time: 68.5 us; the launch traced here: 68.4 us
  Pallas kernels  67.7 us (99%)
    pallas_call x1, Pallas kernels, per_device(): pl.pallas_call(functools.partial(kernel, n_tp, n_ep), out_shape=shapes, i...  67.1 us

profile of v8, /device:TPU:1, one launch (start us, length us, event | category | flops | bytes accessed | tf_op | source)
XLA Modules:
  0.0 68.4 jit_solution(17951786476451868774)
XLA Ops:
  0.6 67.1 %shard_map.211 = (bf16[32,256]{1,0:T(8,128)(2,1)S(1)}, bf16[2,256]{1,0:T(2,128)(2,1)S(1)}, bf16[2,64]{1,0:T(2,128)(2,1)S(1)}) custom-call(bf16[2,4096]{1,0:T(2,128)(2,1)} %tokens.1, s32[1,32]{1,0:T(1,128)} %bitcast.15, bf16[2,1024,256]{2,1,0:T(8,128)(2,1)} %latent_cache.1, bf16[2,64,1024]{2,1,0:T(8,128)(2,1)} %bitcast.9, bf16[4096]{0:T(1024)(128)(2,1)} %attn_gain.1, ...), custom_call_target="tpu_custom_call" | custom-call | tf_op jit(solution)/shard_map/pallas_call | solution.py:795
  67.7 0.6 shard_map.212
